TPU v7x, 256 devices: a 4x2x16 block of a 4x16x16 slice. The times are simulated.
256 devices in a mesh: grp: 2 (over y), ep: 32 (over z, core), tp: 4 (over x).
Axes of the slice: x: 4, y: 2, z: 16, core: 2. Of those that a mesh axis runs over, the one named last changes fastest.
The devices are a block of a 4x16x16 slice.
Arguments:
- x_in: bfloat16 [4096, 2048], P(('grp', 'ep')), parts along dimension 0, may hold values from -6 to 6
- state: float32 [4096, 96, 128], P(('grp', 'ep'), 'tp'), parts along dimension 0, may hold values from -6 to 6
- routes: int32 [4096, 2], P(('grp', 'ep')), parts along dimension 0, may hold values from 0 to 63, as said below
- w_in: bfloat16 [2048, 1536], P(None, 'tp'), may hold values from -0.125 to 0.125
- decay_rate: float32 [96, 64], P('tp'), may hold values from 0.01 to 1
- frequency: float32 [96, 64], P('tp'), may hold values from 0 to 192
- log_step: float32 [96], P('tp'), may hold values from -3 to 0
- b_in: float32 [96, 16, 128], P('tp'), may hold values from -1.5 to 1.5
- c_out: float32 [96, 16, 128], P('tp'), may hold values from -0.5 to 0.5
- skip: float32 [1536], P('tp'), may hold values from -3 to 3
- w_out: bfloat16 [1536, 2048], P('tp'), may hold values from -0.15625 to 0.15625
- gain_mix: float32 [2048], replicated, may hold values from 0.1 to 1.9
- w_group: bfloat16 [2048, 4], replicated, may hold values from -0.0625 to 0.0625
- w_expert: bfloat16 [2048, 64], replicated, may hold values from -0.0625 to 0.0625
- w_gate: bfloat16 [64, 2048, 1024], P('ep', None, 'tp'), may hold values from -0.125 to 0.125
- w_up: bfloat16 [64, 2048, 1024], P('ep', None, 'tp'), may hold values from -0.125 to 0.125
- w_down: bfloat16 [64, 1024, 2048], P('ep', 'tp'), may hold values from -3 to 3
- gain_moe: float32 [2048], replicated, may hold values from 0.1 to 1.9
Outputs:
- layer_out: bfloat16 [4096, 2048], P(('grp', 'ep')), parts along dimension 0
- new_state: float32 [4096, 96, 128], P(('grp', 'ep'), 'tp'), parts along dimension 0
There are 2 independent parts, one for each index of `grp`. A program takes and returns all parts, laid end to end along the dimension named above; an argument that names none is the same for every part. Nothing has to cross between parts.
Inputs may be any that keep to these rules, and one draw needn't show every extreme that they name: `routes`: each row names two different experts of one group of 16 consecutive expert numbers. Within the rows of one index of ep (aligned blocks of 64 rows) no expert is named by more than 4 rows, and in every block some expert is named by exactly 4 rows.
All inputs are finite; a program needn't handle non-finite values.
Results may differ from a plain program's by a relative error of at most 0.015.
Values may be sent and summed in bfloat16 or wider, within the bound.
A program may use at most 64 MiB of HBM per device.

v0:
```python
import jax
import jax.numpy as jnp
from jax import lax
from jax.sharding import PartitionSpec as P

residual_scale = 8.0**0.25
norm_eps = 1e-05


def sent_to_all(x, axis):
    devices = lax.axis_size(axis)
    return lax.all_to_all(jnp.broadcast_to(x[None], (devices, *x.shape)), axis, 0, 0, tiled=True)


def taken_together(x, axis):
    everything = sent_to_all(x, axis)
    return jnp.sum(everything.astype(jnp.float32), axis=0)


def in_order(parts, dim):
    lengths = list(parts.shape[1:])
    lengths[dim] *= parts.shape[0]
    return jnp.moveaxis(parts, 0, dim).reshape(lengths)


def gather_directly(x, axis, dim):
    parts = sent_to_all(x, axis)
    return in_order(parts, dim)


def split_up(x, dim, devices):
    before, after = (x.shape[:dim], x.shape[dim + 1 :])
    return jnp.moveaxis(x.reshape(*before, devices, -1, *after), dim, 0)


def sent_and_summed(x, axis, dim):
    devices = lax.axis_size(axis)
    parts = lax.all_to_all(split_up(x, dim, devices), axis, 0, 0, tiled=True)
    return jnp.sum(parts.astype(jnp.float32), axis=0)


def normalize(values, gain):
    centre = jnp.mean(values, -1, keepdims=True)
    spread = jnp.mean(jnp.square(values - centre), -1, keepdims=True)
    return (values - centre) * lax.rsqrt(spread + norm_eps) * gain


def s5_advance(mix_input, state, decay_rate, frequency, log_step, b_in, c_out, skip):
    top_precision = lax.Precision.DEFAULT
    entries = decay_rate.shape[-1]
    group_count = decay_rate.shape[0]
    width = b_in.shape[1]
    seq_count = mix_input.shape[0]
    input_rows = mix_input.astype(jnp.float32).reshape(seq_count, group_count, width)
    step_size = jnp.exp(log_step)[:, None]
    lam_real = -decay_rate
    magnitude = jnp.exp(lam_real * step_size)
    angle_dt = frequency * step_size
    bar_real = magnitude * jnp.cos(angle_dt)
    bar_imag = magnitude * jnp.sin(angle_dt)
    minus_real = bar_real - 1.0
    modulus = lam_real * lam_real + frequency * frequency
    ratio_real = (minus_real * lam_real + bar_imag * frequency) / modulus
    ratio_imag = (bar_imag * lam_real - minus_real * frequency) / modulus
    in_real = b_in[..., :entries]
    in_imag = b_in[..., entries:]
    input_matrix_real = ratio_real[:, None, :] * in_real - ratio_imag[:, None, :] * in_imag
    input_matrix_imag = ratio_real[:, None, :] * in_imag + ratio_imag[:, None, :] * in_real
    forcing_real = jnp.einsum(
        "rxf,xfb->rxb", input_rows, input_matrix_real, precision=top_precision
    )
    forcing_imag = jnp.einsum(
        "rxf,xfb->rxb", input_rows, input_matrix_imag, precision=top_precision
    )
    old_real = state[..., :entries]
    old_imag = state[..., entries:]
    following_real = bar_real * old_real - bar_imag * old_imag + forcing_real
    following_imag = bar_real * old_imag + bar_imag * old_real + forcing_imag
    output_real = c_out[..., :entries]
    output_imag = c_out[..., entries:]
    output_matrix = jnp.einsum("lzt,zft->lzf", following_real, output_real, precision=top_precision)
    output_matrix = output_matrix - jnp.einsum(
        "lzt,zft->lzf", following_imag, output_imag, precision=top_precision
    )
    output_matrix = output_matrix + skip.reshape(group_count, width) * input_rows
    activated = jax.nn.gelu(output_matrix).reshape(seq_count, group_count * width)
    return (activated, jnp.concatenate([following_real, following_imag], axis=-1))


def route_weights(normed, routes, w_group, w_expert):
    group_total = w_group.shape[1]
    expert_total = w_expert.shape[1]
    per_group = expert_total // group_total
    group_logit = jnp.dot(normed, w_group, preferred_element_type=jnp.float32)
    group_exp = jnp.exp(group_logit)
    group_prob = group_exp / jnp.sum(group_exp, -1, keepdims=True)
    chosen = routes[:, 0] // per_group
    group_pick = jnp.sum(
        jnp.where(
            chosen[:, None] == jnp.arange(group_total, dtype=jnp.int32)[None, :], group_prob, 0.0
        ),
        -1,
    )
    expert_logit = jnp.dot(normed, w_expert, preferred_element_type=jnp.float32)
    picked = jnp.sum(
        jnp.where(
            routes[:, :, None] == jnp.arange(expert_total, dtype=jnp.int32)[None, None, :],
            expert_logit[:, None, :],
            0.0,
        ),
        -1,
    )
    pair_exp = jnp.exp(picked)
    return pair_exp / jnp.sum(pair_exp, -1, keepdims=True) * group_pick[:, None]


def per_device(
    x_in,
    state,
    routes,
    w_in,
    decay_rate,
    frequency,
    log_step,
    b_in,
    c_out,
    skip,
    w_out,
    gain_mix,
    w_group,
    w_expert,
    w_gate,
    w_up,
    w_down,
    gain_moe,
):
    top_precision = lax.Precision.DEFAULT
    seq_count = x_in.shape[0]
    model_width = x_in.shape[1]
    mix_input = jnp.dot(x_in, w_in, preferred_element_type=jnp.float32).astype(jnp.bfloat16)
    activated, new_state = s5_advance(
        mix_input, state, decay_rate, frequency, log_step, b_in, c_out, skip
    )
    partial_mix = jnp.dot(activated.astype(jnp.bfloat16), w_out, preferred_element_type=jnp.float32)
    mixed = taken_together(partial_mix.astype(jnp.bfloat16), "tp").astype(jnp.float32)
    hidden_state = normalize(residual_scale * x_in.astype(jnp.float32) + mixed, gain_mix)
    hidden_bf = hidden_state.astype(jnp.bfloat16)
    route_weight = route_weights(hidden_bf, routes, w_group, w_expert)
    expert_total = w_expert.shape[1]
    ep_count = lax.axis_size("ep")
    local_experts = w_gate.shape[0]
    capacity = max(2, 4 * seq_count // expert_total)
    total_slots = expert_total * capacity
    hits = (routes[:, :, None] == jnp.arange(expert_total, dtype=jnp.int32)[None, None, :]).astype(
        jnp.int32
    )
    tally = jnp.sum(hits, axis=1)
    prior = jnp.cumsum(tally, axis=0) - tally
    slot_in_block = jnp.sum(prior[:, None, :] * hits, axis=-1)
    target = routes * capacity + slot_in_block
    slot_ids = jnp.arange(total_slots, dtype=jnp.int32)
    matches = target[:, :, None] == slot_ids[None, None, :]
    dispatch_map = jnp.any(slot_ids[:, None, None] == target[None, :, :], axis=-1).astype(
        jnp.bfloat16
    )
    combine_map = jnp.sum(jnp.where(matches, route_weight[:, :, None], 0.0), axis=1)
    buffer = jnp.dot(dispatch_map, hidden_bf, preferred_element_type=jnp.float32).astype(
        jnp.bfloat16
    )
    buffer = buffer.reshape(ep_count, local_experts, capacity, model_width)
    column_width = model_width // lax.axis_size("tp")
    own_columns = lax.dynamic_slice_in_dim(
        buffer, lax.axis_index("tp") * column_width, column_width, 3
    )
    piece = gather_directly(
        lax.all_to_all(own_columns, "ep", split_axis=0, concat_axis=0, tiled=True), "tp", 3
    )
    gate_part = jnp.einsum("njcd,jdf->njcf", piece, w_gate, preferred_element_type=jnp.float32)
    up_part = jnp.einsum("njcd,jdf->njcf", piece, w_up, preferred_element_type=jnp.float32)
    act = (jax.nn.silu(gate_part) * up_part).astype(jnp.bfloat16)
    share = sent_and_summed(
        jnp.einsum("njcf,jfd->njcd", act, w_down, preferred_element_type=jnp.float32).astype(
            jnp.bfloat16
        ),
        "tp",
        3,
    ).astype(jnp.bfloat16)
    returned_rows = lax.all_to_all(share, "ep", split_axis=0, concat_axis=0, tiled=True)
    flat_rows = returned_rows.reshape(total_slots, returned_rows.shape[3])
    moe = jnp.dot(
        combine_map,
        lax.all_gather(flat_rows, "tp", axis=1, tiled=True).astype(jnp.float32),
        precision=top_precision,
    )
    layer_out = normalize(residual_scale * hidden_state + moe, gain_moe).astype(jnp.bfloat16)
    return (layer_out, new_state)


def solution(mesh):
    in_specs = (
        P(("grp", "ep"), None),
        P(("grp", "ep"), "tp", None),
        P(("grp", "ep"), None),
        P(None, "tp"),
        P("tp", None),
        P("tp", None),
        P("tp"),
        P("tp", None, None),
        P("tp", None, None),
        P("tp"),
        P("tp", None),
        P(),
        P(),
        P(),
        P("ep", None, "tp"),
        P("ep", None, "tp"),
        P("ep", "tp", None),
        P(),
    )
    out_specs = (P(("grp", "ep"), None), P(("grp", "ep"), "tp", None))
    return jax.shard_map(
        per_device, mesh=mesh, in_specs=in_specs, out_specs=out_specs, check_vma=False
    )
```

profile of v0, /device:TPU:40, one launch (start us, length us, event | category | flops | bytes accessed | tf_op | source)
XLA Modules:
  0.0 197.4 jit_solution(56538877208457532)
XLA Ops:
  8.0 1.9 convolution_convert_fusion.3
  11.4 1.4 fusion.6
  12.9 1.6 fusion.41
  15.3 1.2 broadcast_in_dim.24
  16.4 4.6 %all-to-all-start = ((bf16[4,64,2048]{2,1,0:T(8,128)(2,1)}), bf16[4,64,2048]{2,1,0:T(8,128)(2,1)}, u32[]{:S(2)}, u32[]{:S(2)}) async-start(bf16[4,64,2048]{2,1,0:T(8,128)(2,1)} %broadcast_in_dim.24), calls=%async_computation | async-start | bytes 2097152 | tf_op jit(solution)/shard_map/all_to_all | solution.py:12
  21.5 14.8 %all-to-all-done = bf16[4,64,2048]{2,1,0:T(8,128)(2,1)} async-done(((bf16[4,64,2048]{2,1,0:T(8,128)(2,1)}), bf16[4,64,2048]{2,1,0:T(8,128)(2,1)}, u32[]{:S(2)}, u32[]{:S(2)}) %all-to-all-start) | async-done | bytes 1048608 | tf_op jit(solution)/shard_map/all_to_all | solution.py:12
  36.3 1.4 convert_reduce_fusion
  38.8 1.2 multiply_reduce_fusion.1
  41.8 1.5 convolution_convert_fusion.1
  43.3 2.3 %reshape.109 = bf16[32,2,4,2048]{3,2,1,0:T(4,128)(2,1)} reshape(bf16[256,2048]{1,0:T(8,128)(2,1)} %convolution_convert_fusion.1) | data formatting | bytes 2097152 | tf_op jit(solution)/shard_map/reshape | solution.py:170
  46.6 46.5 %all_to_all.25 = bf16[32,2,4,512]{3,2,1,0:T(4,128)(2,1)S(1)} all-to-all(bf16[32,2,4,512]{3,2,1,0:T(4,128)(2,1)S(1)} %constant_dynamic-slice_fusion), channel_id=1, replica_groups=mesh['grp'=2,'ep'=32,'tp'=4] {'ep'}, dimensions={0} | all-to-all | bytes 524288 | tf_op jit(solution)/shard_map/all_to_all | solution.py:176
  93.4 18.0 %all_to_all.26 = bf16[4,32,2,4,512]{4,1,3,2,0:T(8,128)(2,1)S(1)} all-to-all(bf16[4,32,2,4,512]{4,1,3,2,0:T(8,128)(2,1)S(1)} %broadcast_in_dim.34), channel_id=1, replica_groups=mesh['grp'=2,'ep'=32,'tp'=4] {'tp'}, dimensions={0} | all-to-all | bytes 2097152 | tf_op jit(solution)/shard_map/all_to_all | solution.py:12
  112.6 1.2 fusion.7
  113.7 3.8 %convolution_convert_fusion = bf16[2,32,4,2048]{3,1,2,0:T(8,128)(2,1)} fusion(bf16[2,256,2048]{2,1,0:T(8,128)(2,1)S(1)} %copy-done, bf16[32,2,4,2048]{3,0,2,1:T(8,128)(2,1)} %bitcast.85, bf16[2,2048,256]{2,1,0:T(8,128)(2,1)} %param.33, f32[32,2,4,256]{3,0,2,1:T(8,128)} %fusion.7), kind=kOutput, calls=%fused_computation | convolution fusion | flops 537788416 | bytes 6553600 | tf_op jit(solution)/shard_map/njcf,jfd->njcd/dot_general | solution.py:182
  117.5 1.4 copy.95
  118.8 17.5 %all_to_all.27 = bf16[4,32,2,4,512]{4,1,3,2,0:T(8,128)(2,1)} all-to-all(bf16[4,32,2,4,512]{4,1,3,2,0:T(8,128)(2,1)S(1)} %bitcast.88), channel_id=1, replica_groups=mesh['grp'=2,'ep'=32,'tp'=4] {'tp'}, dimensions={0} | all-to-all | bytes 2097152 | tf_op jit(solution)/shard_map/all_to_all | solution.py:38
  136.3 2.2 %reduce_sum.130 = bf16[32,2,4,512]{3,0,2,1:T(8,128)(2,1)} reduce(bf16[4,32,2,4,512]{4,1,3,2,0:T(8,128)(2,1)} %all_to_all.27, bf16[]{:T(256)} %constant.58.clone.1), dimensions={0}, to_apply=%region_12.13 | reduce | flops 393216 | bytes 1310722 | tf_op jit(solution)/shard_map/reduce_sum | solution.py:39
  138.5 1.2 copy.80
  139.7 26.5 %all_to_all.28 = bf16[32,2,4,512]{3,2,1,0:T(4,128)(2,1)} all-to-all(bf16[32,2,4,512]{3,2,1,0:T(4,128)(2,1)S(1)} %copy.80), channel_id=1, replica_groups=mesh['grp'=2,'ep'=32,'tp'=4] {'ep'}, dimensions={0} | all-to-all | bytes 524288 | tf_op jit(solution)/shard_map/all_to_all | solution.py:188
  166.2 1.7 reshape.112
  168.0 1.5 pad_maximum_fusion
  169.5 1.3 copy.81
  171.7 16.1 %all-gather.2.cloned.1.call-done = bf16[256,2048]{1,0:T(8,128)(2,1)} async-done(((bf16[256,512]{1,0:T(8,128)(2,1)}), bf16[256,2048]{1,0:T(8,128)(2,1)}) %all-gather.2.cloned.1.call-update) | async-done | bytes 1048592 | tf_op jit(solution)/shard_map/all_gather | solution.py:192
  187.8 1.7 fusion.62
  (72 shorter events, 10.8 us)
Async XLA Ops:
  7.2 106.6 %copy-start = (bf16[2,256,2048]{2,1,0:T(8,128)(2,1)S(1)}, bf16[2,256,2048]{2,1,0:T(8,128)(2,1)}, u32[]{:S(2)}) copy-start(bf16[2,256,2048]{2,1,0:T(8,128)(2,1)} %param.34) | copy-start | bytes 6291460
  7.2 2.9 %copy-start.5 = (f32[64,24,128]{2,1,0:T(8,128)S(1)}, f32[64,24,128]{2,1,0:T(8,128)}, u32[]{:S(2)}) copy-start(f32[64,24,128]{2,1,0:T(8,128)} %param.19) | copy-start | bytes 2359300
  9.9 0.7 copy-start.14
  9.9 0.7 copy-start.15
  9.9 0.9 copy-start.9
  10.9 1.9 copy-start.17
  10.9 2.0 %copy-start.8 = (f32[24,16,128]{2,1,0:T(8,128)S(1)}, f32[24,16,128]{2,1,0:T(8,128)}, u32[]{:S(2)}) copy-start(f32[24,16,128]{2,1,0:T(8,128)} %param.26) | copy-start | bytes 589828
  12.9 2.0 %copy-start.7 = (bf16[384,2048]{1,0:T(8,128)(2,1)S(1)}, bf16[384,2048]{1,0:T(8,128)(2,1)}, u32[]{:S(2)}) copy-start(bf16[384,2048]{1,0:T(8,128)(2,1)} %param.28) | copy-start | bytes 4718596
  15.3 5.8 %copy-start.13 = (s32[64,2]{0,1:T(2,128)S(1)}, s32[64,2]{0,1:T(2,128)}, u32[]{:S(2)}) copy-start(s32[64,2]{0,1:T(2,128)} %param.20) | copy-start | bytes 1540
  16.4 19.8 %all-to-all-start = ((bf16[4,64,2048]{2,1,0:T(8,128)(2,1)}), bf16[4,64,2048]{2,1,0:T(8,128)(2,1)}, u32[]{:S(2)}, u32[]{:S(2)}) async-start(bf16[4,64,2048]{2,1,0:T(8,128)(2,1)} %broadcast_in_dim.24), calls=%async_computation | async-start | bytes 2097152 | tf_op jit(solution)/shard_map/all_to_all | solution.py:12
  21.0 19.0 %copy-start.11 = (f32[2048]{0:T(1024)S(1)}, f32[2048]{0:T(1024)}, u32[]{:S(2)}) copy-start(f32[2048]{0:T(1024)} %param.29) | copy-start | bytes 24580
  21.0 166.7 %all-gather.2.cloned.1.call-start = ((), (), s32[]{:S(2)}) async-start(), calls=%async_computation.5 | async-start | bytes 1310720 | tf_op jit(solution)/shard_map/all_gather | solution.py:192
  41.1 0.7 copy-start.3
  93.4 19.2 %copy-start.6 = (bf16[2,2048,256]{2,1,0:T(8,128)(2,1)S(1)}, bf16[2,2048,256]{2,1,0:T(8,128)(2,1)}, u32[]{:S(2)}) copy-start(bf16[2,2048,256]{2,1,0:T(8,128)(2,1)} %param.32) | copy-start | bytes 6291460
  111.6 1.0 copy-start.1
  168.0 2.9 %copy-start.4 = (bf16[64,2048]{1,0:T(8,128)(2,1)S(1)}, bf16[64,2048]{1,0:T(8,128)(2,1)}, u32[]{:S(2)}) copy-start(bf16[64,2048]{1,0:T(8,128)(2,1)} %copy-done.3) | copy-start | bytes 786436
  168.0 2.9 %copy-start.10 = (bf16[2048,64]{0,1:T(8,128)(2,1)S(1)}, bf16[2048,64]{0,1:T(8,128)(2,1)}, u32[]{:S(2)}) copy-start(bf16[2048,64]{0,1:T(8,128)(2,1)} %param.31) | copy-start | bytes 786436
  168.0 3.3 %copy-start.12 = (bf16[2048,4]{0,1:T(4,128)(2,1)S(1)}, bf16[2048,4]{0,1:T(4,128)(2,1)}, u32[]{:S(2)}) copy-start(bf16[2048,4]{0,1:T(4,128)(2,1)} %param.30) | copy-start | bytes 49156
  169.5 18.3 %copy-start.2 = (bf16[64,2048]{1,0:T(8,128)(2,1)S(1)}, bf16[64,2048]{1,0:T(8,128)(2,1)}, u32[]{:S(2)}) copy-start(bf16[64,2048]{1,0:T(8,128)(2,1)} %param.18) | copy-start | bytes 786436
  170.8 18.8 %copy-start.16 = (f32[2048]{0:T(1024)S(1)}, f32[2048]{0:T(1024)}, u32[]{:S(2)}) copy-start(f32[2048]{0:T(1024)} %param.35) | copy-start | bytes 24580
Sparse Core Ops, SparseCore 0:
  168.1 19.5 all-gather.1
where the time goes:
time: 198 us; the launch traced here: 197 us
  blocking collectives  109 us (55%)
  waiting for transfers between devices  30.9 us (16%)
  matrix products  14.6 us (7%)
  between operations  14.4 us (7%)
  local copies, waits for them, and re-layouts  13.8 us (7%)
  other arithmetic  10.5 us (5%)
  starting transfers between devices  4.58 us (2%)
    all_to_all x1, blocking collectives, per_device(): lax.all_to_all(own_columns, 'ep', split_axis=0, concat_axis=0, tiled=True)  46.5 us
    all_to_all x1, blocking collectives, per_device(): lax.all_to_all(share, 'ep', split_axis=0, concat_axis=0, tiled=True)  26.5 us
    all_to_all x1, blocking collectives, sent_to_all(): lax.all_to_all(jnp.broadcast_to(x[None], (devices, *x.shape)), axis, 0, 0...  18 us
    all_to_all x1, blocking collectives, sent_and_summed(): parts = lax.all_to_all(split_up(x, dim, devices), axis, 0, 0, tiled=True)  17.5 us
    all_gather x1, waiting for transfers between devices, per_device(): lax.all_gather(flat_rows, 'tp', axis=1, tiled=True).astype(jnp.float32)  16.1 us
    all_to_all x1, waiting for transfers between devices, sent_to_all(): lax.all_to_all(jnp.broadcast_to(x[None], (devices, *x.shape)), axis, 0, 0...  14.8 us
    all_to_all x1, starting transfers between devices, sent_to_all(): lax.all_to_all(jnp.broadcast_to(x[None], (devices, *x.shape)), axis, 0, 0...  4.58 us
  transfers between devices with their start and end apart: 2, of which 2 were waited for; matrix products, arithmetic and copies ran while one was open for 2% of the time, Pallas kernels for 0%

commit v1 on v0

v1 whole, which is shorter than its diff:
```python
import functools

import jax
import jax.numpy as jnp
from jax import lax
from jax.experimental import pallas as pl
from jax.experimental.pallas import tpu as pltpu
from jax.sharding import PartitionSpec as P

residual_scale = 8.0**0.25
norm_eps = 1e-05
CORES = 2
CHUNKS = 4
F32 = jnp.float32
BF16 = jnp.bfloat16
MESH = pl.DeviceIdType.MESH


def dot(a, b):
    return jnp.dot(a, b, preferred_element_type=F32)


def chip_offsets(chips):
    order = [0]
    for step in range(1, chips // 2):
        order += [step, chips - step]
    order.append(chips // 2)
    size = chips // CHUNKS
    return [order[k * size : (k + 1) * size] for k in range(CHUNKS)]


def layer_kernel(
    n_ep,
    n_tp,
    x_h,
    state_h,
    routes_h,
    win_h,
    decay_h,
    freq_h,
    lstep_h,
    b_h,
    c_h,
    skip_h,
    wout_h,
    gmix_h,
    wgrp_h,
    wexp_h,
    wg_h,
    wu_h,
    wd_h,
    gmoe_h,
    out_h,
    ns_h,
    x_v,
    state_v,
    routes_v,
    win_v,
    decay_v,
    freq_v,
    lstep_v,
    b_v,
    c_v,
    skip_v,
    wout_v,
    gmix_v,
    wgrp_v,
    wexp_v,
    wg_v,
    wu_v,
    wd_v,
    gmoe_v,
    ns_v,
    out_part,
    out_recv,
    hid_v,
    stat_send,
    stat_recv,
    z_buf,
    z_recv_buf,
    gather_buf,
    down_part,
    down_recv,
    ret_send,
    ret_buf,
    fin_v,
    load_sem,
    store_sem,
    a_send,
    a_recv,
    s_send,
    s_recv,
    z_send,
    z_recv,
    x_send,
    x_recv,
    d_send,
    d_recv,
    r_send,
    r_recv,
    f_send,
    f_recv,
):
    ep = lax.axis_index("ep")
    tp = lax.axis_index("tp")
    chips = n_ep // CORES
    chip = ep // CORES
    core = ep % CORES
    rows, width = x_v.shape
    share = width // n_tp
    entries = decay_v.shape[1]
    lanes = 2 * entries
    groups = decay_v.shape[0]
    group_width = b_v.shape[0] // groups
    experts = wexp_v.shape[1]
    egroups = wgrp_v.shape[1]
    local_experts = wg_v.shape[0]
    cap = z_buf.shape[1] // local_experts
    slots = z_buf.shape[1]
    offsets = chip_offsets(chips)
    per_chunk = n_ep // CHUNKS
    chunk_rows = per_chunk * slots
    share_at = pl.ds(pl.multiple_of(tp * share, share), share)

    barrier = pltpu.get_barrier_semaphore()

    def greet_ep(i, _):
        peer = (ep + i) % n_ep
        pl.semaphore_signal(barrier, inc=1, device_id={"ep": peer}, device_id_type=MESH)
        return 0

    for r in range(1, n_tp):
        pl.semaphore_signal(
            barrier, inc=1, device_id={"tp": (tp + r) % n_tp}, device_id_type=MESH
        )
    lax.fori_loop(1, n_ep, greet_ep, 0)

    loads = {}
    pairs = (
        ("x", x_h, x_v),
        ("win", win_h, win_v),
        ("decay", decay_h, decay_v),
        ("freq", freq_h, freq_v),
        ("lstep", lstep_h, lstep_v),
        ("b", b_h, b_v),
        ("c", c_h, c_v),
        ("state", state_h, state_v),
        ("skip", skip_h, skip_v),
        ("wout", wout_h, wout_v),
        ("gmix", gmix_h.at[:, share_at], gmix_v),
        ("routes", routes_h, routes_v),
        ("wgrp", wgrp_h.at[share_at, :], wgrp_v),
        ("wexp", wexp_h.at[share_at, :], wexp_v),
        ("wg", wg_h, wg_v),
        ("wu", wu_h, wu_v),
        ("wd", wd_h, wd_v),
        ("gmoe", gmoe_h.at[:, share_at], gmoe_v),
    )
    for i, (name, src, dst) in enumerate(pairs):
        loads[name] = pltpu.make_async_copy(src, dst, load_sem.at[i])
        loads[name].start()

    sends = []

    def send(src, dst, send_sem, recv_sem, target):
        copy = pltpu.make_async_remote_copy(
            src_ref=src,
            dst_ref=dst,
            send_sem=send_sem,
            recv_sem=recv_sem,
            device_id=target,
            device_id_type=MESH,
        )
        copy.start()
        sends.append(copy)
        return copy

    for name in ("decay", "freq", "lstep", "b", "c"):
        loads[name].wait()
    eye = (
        lax.broadcasted_iota(jnp.int32, (groups, groups), 0)
        == lax.broadcasted_iota(jnp.int32, (groups, groups), 1)
    )
    log_step = jnp.sum(jnp.where(eye, lstep_v[...], 0.0), axis=1, keepdims=True)
    step_size = jnp.exp(log_step)
    decay = decay_v[...]
    freq = freq_v[...]
    lam_real = -decay
    magnitude = jnp.exp(lam_real * step_size)
    angle = freq * step_size
    bar_real = magnitude * jnp.cos(angle)
    bar_imag = magnitude * jnp.sin(angle)
    minus_real = bar_real - 1.0
    modulus = lam_real * lam_real + freq * freq
    ratio_real = (minus_real * lam_real + bar_imag * freq) / modulus
    ratio_imag = (bar_imag * lam_real - minus_real * freq) / modulus
    bar_same = jnp.concatenate([bar_real, bar_real], axis=1)
    bar_cross = jnp.concatenate([-bar_imag, bar_imag], axis=1)
    ratio_same = jnp.concatenate([ratio_real, ratio_real], axis=1)
    ratio_cross = jnp.concatenate([-ratio_imag, ratio_imag], axis=1)

    loads["x"].wait()
    loads["win"].wait()
    mix_input = dot(x_v[...], win_v[...]).astype(BF16)
    loads["skip"].wait()
    loads["state"].wait()

    per_block = lanes // group_width
    block_lanes = per_block * lanes
    own_group = (
        lax.broadcasted_iota(jnp.int32, (lanes, block_lanes), 0) // group_width
        == lax.broadcasted_iota(jnp.int32, (lanes, block_lanes), 1) // lanes
    )
    sign = jnp.where(lax.broadcasted_iota(jnp.int32, (1, lanes), 1) < entries, 1.0, -1.0)
    acts = []
    for j in range(groups // per_block):
        channels = slice(j * lanes, (j + 1) * lanes)
        bars = []
        for g in range(j * per_block, (j + 1) * per_block):
            b_g = b_v[g * group_width : (g + 1) * group_width, :]
            bars.append(
                b_g * ratio_same[g : g + 1, :]
                + pltpu.roll(b_g, entries, 1) * ratio_cross[g : g + 1, :]
            )
        b_bar = jnp.concatenate(bars, axis=0)
        b_wide = jnp.where(own_group, jnp.concatenate([b_bar] * per_block, axis=1), 0.0)
        u_j = mix_input[:, channels]
        forcing = dot(u_j, b_wide.astype(BF16))
        news = []
        for i in range(per_block):
            g = j * per_block + i
            old = state_v[pl.ds(g, rows, stride=groups), :]
            new = (
                old * bar_same[g : g + 1, :]
                + pltpu.roll(old, entries, 1) * bar_cross[g : g + 1, :]
                + forcing[:, i * lanes : (i + 1) * lanes]
            )
            ns_v[pl.ds(g, rows, stride=groups), :] = new
            news.append(new.astype(BF16))
        c_j = c_v[channels, :] * sign
        c_wide = jnp.where(own_group, jnp.concatenate([c_j] * per_block, axis=1), 0.0)
        y = lax.dot_general(
            jnp.concatenate(news, axis=1),
            c_wide.astype(BF16),
            (((1,), (1,)), ((), ())),
            preferred_element_type=F32,
        )
        y = y + skip_v[:, channels] * u_j.astype(F32)
        acts.append(jax.nn.gelu(y).astype(BF16))
    store = pltpu.make_async_copy(ns_v, ns_h, store_sem)
    store.start()
    act_mix = jnp.concatenate(acts, axis=1)

    loads["wout"].wait()
    pl.semaphore_wait(barrier, n_ep - 1 + n_tp - 1)
    waits = {}
    for r in (2, 1, 3, 0):
        q = (tp + r) % n_tp
        cols = pl.ds(pl.multiple_of(q * share, share), share)
        out_part[r] = dot(act_mix, wout_v[:, cols]).astype(BF16)
        if r:
            waits[r] = send(
                out_part.at[r], out_recv.at[r - 1], a_send.at[r - 1], a_recv.at[r - 1], {"tp": q}
            )

    for name in ("routes", "gmix", "wgrp", "wexp"):
        loads[name].wait()
    route = [routes_v[:, k : k + 1] for k in range(2)]
    expert_id = lax.broadcasted_iota(jnp.int32, (rows, experts), 1)
    chosen = [(route[k] == expert_id).astype(F32) for k in range(2)]
    hits = chosen[0] + chosen[1]
    row_id = lax.broadcasted_iota(jnp.int32, (rows, rows), 0)
    col_id = lax.broadcasted_iota(jnp.int32, (rows, rows), 1)
    earlier = (row_id > col_id).astype(BF16)
    prior = dot(earlier, hits.astype(BF16))
    slot_id = lax.broadcasted_iota(jnp.int32, (rows, experts * cap), 1).astype(F32)
    places = []
    for k in range(2):
        rank = jnp.sum(prior * chosen[k], axis=1, keepdims=True)
        target = route[k].astype(F32) * cap + rank
        places.append((target == slot_id).astype(F32))
    dispatch_map = (places[0] + places[1]).astype(BF16)

    diagonal = (
        lax.broadcasted_iota(jnp.int32, (rows, 128), 0)
        == lax.broadcasted_iota(jnp.int32, (rows, 128), 1)
    )

    def exchange(n, columns):
        for i, column in enumerate(columns):
            stat_send[n, i : i + 1, :] = jnp.sum(
                jnp.where(diagonal, column, 0.0), axis=0, keepdims=True
            )
        for r in (2, 1, 3):
            send(
                stat_send.at[n],
                stat_recv.at[n, r - 1],
                s_send.at[n, r - 1],
                s_recv.at[n, r - 1],
                {"tp": (tp + r) % n_tp},
            )

    def received(n, count):
        for r in range(1, n_tp):
            pltpu.make_async_copy(
                stat_recv.at[n, r - 1], stat_recv.at[n, r - 1], s_recv.at[n, r - 1]
            ).wait()
        parts = [stat_send[n]] + [stat_recv[n, r - 1] for r in range(1, n_tp)]
        return [
            [
                jnp.sum(jnp.where(diagonal, part[i : i + 1, :], 0.0), axis=1, keepdims=True)
                for i in range(count)
            ]
            for part in parts
        ]

    def norm_terms(n, values):
        mean_own = jnp.mean(values, axis=1, keepdims=True)
        spread_own = jnp.sum(jnp.square(values - mean_own), axis=1, keepdims=True)
        exchange(n, [mean_own, spread_own])
        stats = received(n, 2)
        mean = sum(s[0] for s in stats) / n_tp
        spread = sum(s[1] + share * jnp.square(s[0] - mean) for s in stats) / width
        return mean, lax.rsqrt(spread + norm_eps)

    for r in range(1, n_tp):
        waits[r].wait_recv()
    mixed = out_part[0].astype(F32)
    for r in range(1, n_tp):
        mixed = mixed + out_recv[r - 1].astype(F32)
    values = residual_scale * x_v[:, share_at].astype(F32) + mixed
    mean, scale = norm_terms(0, values)
    hidden = (values - mean) * scale * gmix_v[...]
    hid_v[...] = hidden
    hidden_bf = hidden.astype(BF16)

    z_buf[...] = (
        lax.dot_general(
            dispatch_map, hidden_bf, (((0,), (0,)), ((), ())), preferred_element_type=F32
        )
        .reshape(n_ep, slots, share)
        .astype(BF16)
    )
    z_recv_buf[0, core] = z_buf[ep]
    for k in range(CHUNKS):
        for i, offset in enumerate(offsets[k]):
            for c in (1, 0):
                if offset == 0 and c == 0:
                    continue
                target = ((chip + chips - offset) % chips) * CORES + (core + c) % CORES
                send(
                    z_buf.at[target],
                    z_recv_buf.at[k, i * CORES + core],
                    z_send.at[(k * len(offsets[k]) + i) * CORES + c],
                    z_recv.at[k],
                    {"ep": target},
                )

    group_logit = dot(hidden_bf, wgrp_v[...])
    expert_logit = dot(hidden_bf, wexp_v[...])
    columns = [jnp.sum(chosen[k] * expert_logit, axis=1, keepdims=True) for k in range(2)]
    columns += [group_logit[:, i : i + 1] for i in range(egroups)]
    exchange(1, columns)

    def wait_bytes(ref, sem):
        pltpu.make_async_copy(ref, ref, sem).wait()

    def gather(k):
        count = per_chunk - 1 if k == 0 else per_chunk
        wait_bytes(z_recv_buf.at[k, 0:count], z_recv.at[k])
        for r in (2, 1, 3):
            send(
                z_recv_buf.at[k],
                gather_buf.at[k, tp],
                x_send.at[k, r - 1],
                x_recv.at[k, r - 1],
                {"tp": (tp + r) % n_tp},
            )
        gather_buf[k, tp] = z_recv_buf[k]

    def experts_of(k):
        for r in range(1, n_tp):
            wait_bytes(gather_buf.at[k, 0], x_recv.at[k, r - 1])
        if k == 0:
            for name in ("wg", "wu", "wd"):
                loads[name].wait()
        lhs = [gather_buf[k, t].reshape(chunk_rows, share) for t in range(n_tp)]
        lhs = jnp.concatenate(lhs, axis=1)
        slot = lax.broadcasted_iota(jnp.int32, (chunk_rows, 1), 0) % slots
        acts = []
        for e in range(local_experts):
            gate = dot(lhs, wg_v[e])
            up = dot(lhs, wu_v[e])
            mine = slot // cap == e
            acts.append(jnp.where(mine, jax.nn.silu(gate) * up, 0.0).astype(BF16))
        act = jnp.concatenate(acts, axis=1)
        for r in (2, 1, 3, 0):
            q = (tp + r) % n_tp
            cols = pl.ds(pl.multiple_of(q * share, share), share)
            down_part[k, r] = dot(act, wd_v[:, cols]).astype(BF16)
            if r:
                send(
                    down_part.at[k, r],
                    down_recv.at[k, r - 1],
                    d_send.at[k, r - 1],
                    d_recv.at[k, r - 1],
                    {"tp": q},
                )

    def give_back(k):
        for r in range(1, n_tp):
            wait_bytes(down_recv.at[k, r - 1], d_recv.at[k, r - 1])
        total = down_part[k, 0].astype(F32)
        for r in range(1, n_tp):
            total = total + down_recv[k, r - 1].astype(F32)
        ret_send[k] = total.reshape(per_chunk, slots, share).astype(BF16)
        for i, offset in enumerate(offsets[k]):
            for c in (1, 0):
                to_core = (core + c) % CORES
                if offset == 0 and c == 0:
                    continue
                target = ((chip + offset) % chips) * CORES + to_core
                send(
                    ret_send.at[k, i * CORES + to_core],
                    ret_buf.at[ep],
                    r_send.at[(k * len(offsets[k]) + i) * CORES + c],
                    r_recv,
                    {"ep": target},
                )
        if k == 0:
            ret_buf[ep] = ret_send[0, core]

    gather(0)
    gather(1)
    experts_of(0)
    for k in range(2, CHUNKS):
        gather(k)
        experts_of(k - 1)
        give_back(k - 2)
    experts_of(CHUNKS - 1)
    give_back(CHUNKS - 2)

    parts = received(1, 2 + egroups)
    total = [sum(p[i] for p in parts) for i in range(2 + egroups)]
    pair = [jnp.exp(total[k]) for k in range(2)]
    group_exp = [jnp.exp(total[2 + i]) for i in range(egroups)]
    own = route[0] // (experts // egroups)
    picked = sum(jnp.where(own == i, group_exp[i], 0.0) for i in range(egroups))
    group_prob = picked / sum(group_exp)
    pair_sum = pair[0] + pair[1]
    combine_map = sum(places[k] * (pair[k] / pair_sum * group_prob) for k in range(2))
    combine_map = combine_map.astype(BF16)
    loads["gmoe"].wait()

    give_back(CHUNKS - 1)

    wait_bytes(ret_buf.at[0 : n_ep - 1], r_recv)
    returned = ret_buf[...].reshape(n_ep * slots, share)
    values = residual_scale * hid_v[...] + dot(combine_map, returned)
    mean, scale = norm_terms(2, values)
    fin_v[...] = ((values - mean) * scale * gmoe_v[...]).astype(BF16)
    last = []
    for r in (2, 1, 3):
        last.append(
            send(
                fin_v,
                out_h.at[:, share_at],
                f_send.at[r - 1],
                f_recv.at[r - 1],
                {"tp": (tp + r) % n_tp},
            )
        )
    own_store = pltpu.make_async_copy(fin_v, out_h.at[:, share_at], f_send.at[n_tp - 1])
    own_store.start()
    for copy in last:
        copy.wait_recv()
    own_store.wait()
    store.wait()
    for copy in sends:
        copy.wait_send()


def per_device(
    n_ep,
    n_tp,
    x_in,
    state,
    routes,
    w_in,
    decay_rate,
    frequency,
    log_step,
    b_in,
    c_out,
    skip,
    w_out,
    gain_mix,
    w_group,
    w_expert,
    w_gate,
    w_up,
    w_down,
    gain_moe,
):
    rows, width = x_in.shape
    share = width // n_tp
    groups, entries = decay_rate.shape
    lanes = 2 * entries
    channels = skip.shape[0]
    experts = w_expert.shape[1]
    egroups = w_group.shape[1]
    local_experts, _, hidden_units = w_gate.shape
    cap = max(2, 4 * rows // experts)
    slots = local_experts * cap
    per_chunk = n_ep // CHUNKS
    args = (
        x_in,
        state.reshape(rows * groups, lanes),
        routes,
        w_in,
        decay_rate,
        frequency,
        log_step.reshape(1, groups),
        b_in.reshape(channels, lanes),
        c_out.reshape(channels, lanes),
        skip.reshape(1, channels),
        w_out,
        gain_mix.reshape(1, width),
        w_group,
        w_expert,
        w_gate,
        w_up,
        w_down.reshape(local_experts * hidden_units, width),
        gain_moe.reshape(1, width),
    )
    dma = pltpu.SemaphoreType.DMA
    peers = n_tp - 1
    scratch = [
        pltpu.VMEM((rows, width), BF16),
        pltpu.VMEM((rows * groups, lanes), F32),
        pltpu.VMEM(routes.shape, jnp.int32),
        pltpu.VMEM(w_in.shape, BF16),
        pltpu.VMEM(decay_rate.shape, F32),
        pltpu.VMEM(frequency.shape, F32),
        pltpu.VMEM((1, groups), F32),
        pltpu.VMEM((channels, lanes), F32),
        pltpu.VMEM((channels, lanes), F32),
        pltpu.VMEM((1, channels), F32),
        pltpu.VMEM(w_out.shape, BF16),
        pltpu.VMEM((1, share), F32),
        pltpu.VMEM((share, egroups), BF16),
        pltpu.VMEM((share, experts), BF16),
        pltpu.VMEM(w_gate.shape, BF16),
        pltpu.VMEM(w_up.shape, BF16),
        pltpu.VMEM((local_experts * hidden_units, width), BF16),
        pltpu.VMEM((1, share), F32),
        pltpu.VMEM((rows * groups, lanes), F32),
        pltpu.VMEM((n_tp, rows, share), BF16),
        pltpu.VMEM((peers, rows, share), BF16),
        pltpu.VMEM((rows, share), F32),
        pltpu.VMEM((3, 8, 128), F32),
        pltpu.VMEM((3, peers, 8, 128), F32),
        pltpu.VMEM((n_ep, slots, share), BF16),
        pltpu.VMEM((CHUNKS, per_chunk, slots, share), BF16),
        pltpu.VMEM((CHUNKS, n_tp, per_chunk, slots, share), BF16),
        pltpu.VMEM((CHUNKS, n_tp, per_chunk * slots, share), BF16),
        pltpu.VMEM((CHUNKS, peers, per_chunk * slots, share), BF16),
        pltpu.VMEM((CHUNKS, per_chunk, slots, share), BF16),
        pltpu.VMEM((n_ep, slots, share), BF16),
        pltpu.VMEM((rows, share), BF16),
        dma((len(args),)),
        dma,
        dma((peers,)),
        dma((peers,)),
        dma((3, peers)),
        dma((3, peers)),
        dma((n_ep,)),
        dma((CHUNKS,)),
        dma((CHUNKS, peers)),
        dma((CHUNKS, peers)),
        dma((CHUNKS, peers)),
        dma((CHUNKS, peers)),
        dma((n_ep,)),
        dma,
        dma((n_tp,)),
        dma((peers,)),
    ]
    any_space = pl.BlockSpec(memory_space=pl.ANY)
    out, new_state = pl.pallas_call(
        functools.partial(layer_kernel, n_ep, n_tp),
        out_shape=(
            jax.ShapeDtypeStruct((rows, width), BF16),
            jax.ShapeDtypeStruct((rows * groups, lanes), F32),
        ),
        in_specs=[any_space] * len(args),
        out_specs=(any_space, any_space),
        scratch_shapes=scratch,
        compiler_params=pltpu.CompilerParams(
            collective_id=0, has_side_effects=True, vmem_limit_bytes=60 * 1024 * 1024
        ),
        name="layer",
    )(*args)
    return out, new_state.reshape(state.shape)


def solution(mesh):
    in_specs = (
        P(("grp", "ep"), None),
        P(("grp", "ep"), "tp", None),
        P(("grp", "ep"), None),
        P(None, "tp"),
        P("tp", None),
        P("tp", None),
        P("tp"),
        P("tp", None, None),
        P("tp", None, None),
        P("tp"),
        P("tp", None),
        P(),
        P(),
        P(),
        P("ep", None, "tp"),
        P("ep", None, "tp"),
        P("ep", "tp", None),
        P(),
    )
    out_specs = (P(("grp", "ep"), None), P(("grp", "ep"), "tp", None))
    return jax.shard_map(
        functools.partial(per_device, mesh.shape["ep"], mesh.shape["tp"]),
        mesh=mesh,
        in_specs=in_specs,
        out_specs=out_specs,
        check_vma=False,
    )
```

time: 198 us -> 98.6 us (0.50)
  blocking collectives: 109 us -> 0 us
  Pallas kernels: 0 us -> 86.3 us
  waiting for transfers between devices: 30.9 us -> 0 us
  matrix products: 14.6 us -> 0 us
  between operations: 14.4 us -> 0.64 us
  other arithmetic: 10.5 us -> 0 us
  starting transfers between devices: 4.58 us -> 0 us
  local copies, waits for them, and re-layouts: 13.8 us -> 10.1 us
    all_to_all x4 -> x0, blocking collectives: 109 us -> none  [the longest x1 46.5 us: per_device(): lax.all_to_all(own_columns, 'ep', split_axis=0, concat_axis=0, tiled=True)]
    pallas_call x0 -> x1, Pallas kernels: none -> 86.3 us  [per_device(): pl.pallas_call(functools.partial(layer_kernel, n_ep, n_tp), out_shape=(ja...]
    all_gather x1 -> x0, waiting for transfers between devices: 16.1 us -> none  [per_device(): lax.all_gather(flat_rows, 'tp', axis=1, tiled=True).astype(jnp.float32)]
    all_to_all x1 -> x0, waiting for transfers between devices: 14.8 us -> none  [sent_to_all(): lax.all_to_all(jnp.broadcast_to(x[None], (devices, *x.shape)), axis, 0, 0...]
    dot_general x12 -> x0, matrix products: 14.6 us -> none  [the longest x1 3.75 us: per_device(): jnp.einsum('njcf,jfd->njcd', act, w_down, preferred_element_type=jnp.floa...]
    reduce_sum x11 -> x0, other arithmetic: 6.73 us -> none  [the longest x1 2.18 us: sent_and_summed(): return jnp.sum(parts.astype(jnp.float32), axis=0)]
    unnamed x37 -> x5, local copies, waits for them, and re-layouts: 3.5 us -> 8.84 us
    all_to_all x1 -> x0, starting transfers between devices: 4.58 us -> none  [sent_to_all(): lax.all_to_all(jnp.broadcast_to(x[None], (devices, *x.shape)), axis, 0, 0...]
  transfers between devices with their start and end apart: 2 -> 0, of which waited for: 2 -> 0; matrix products, arithmetic and copies ran while one was open for 2% -> 0% of each run, Pallas kernels for 0% -> 0%
where the time goes in v1:
time: 98.6 us; the launch traced here: 97 us
  Pallas kernels  86.3 us (88%)
  local copies, waits for them, and re-layouts  10.1 us (10%)
    pallas_call x1, Pallas kernels, per_device(): pl.pallas_call(functools.partial(layer_kernel, n_ep, n_tp), out_shape=(ja...  86.3 us
    unnamed x5, local copies, waits for them, and re-layouts  8.84 us

profile of v1, /device:TPU:40, one launch (start us, length us, event | category | flops | bytes accessed | tf_op | source)
XLA Modules:
  0.0 97.0 jit_solution(14918452800731449946)
XLA Ops:
  0.6 1.3 %reshape.35.skip_h = f32[1,384]{1,0:T(1,128)} reshape(f32[384]{0:T(512)} %param.27) | data formatting | bytes 3072 | tf_op jit(solution)/shard_map/reshape | solution.py:526
  1.9 1.4 %copy.20.routes_h = s32[64,2]{1,0:T(8,128)} copy(s32[64,2]{0,1:T(2,128)} %param.20) | data formatting | bytes 1024 | tf_op args[2]
  3.3 1.8 %copy.21.wgrp_h = bf16[2048,4]{1,0:T(8,128)(2,1)} copy(bf16[2048,4]{0,1:T(4,128)(2,1)} %param.30) | data formatting | bytes 32768 | tf_op args[12]
  5.0 2.0 %copy.22.wexp_h = bf16[2048,64]{1,0:T(8,128)(2,1)} copy(bf16[2048,64]{0,1:T(8,128)(2,1)} %param.31) | data formatting | bytes 524288 | tf_op args[13]
  7.0 86.3 %layer.1 = (bf16[64,2048]{1,0:T(8,128)(2,1)}, f32[1536,128]{1,0:T(8,128)}) custom-call(bf16[64,2048]{1,0:T(8,128)(2,1)} %x_h.1, f32[1536,128]{1,0:T(8,128)} %bitcast.9, s32[64,2]{1,0:T(8,128)} %copy.20.routes_h, bf16[2048,384]{1,0:T(8,128)(2,1)} %win_h.1, f32[24,64]{1,0:T(8,128)} %decay_h.1, f32[24,64]{1,0:T(8,128)} %freq_h.1, f32[1,24]{1,0:T(1,128)} %bitcast.15, ...), custom_call_target="tpu_custom_call" | custom-call | tf_op jit(solution)/shard_map/layer/pallas_call | solution.py:589
  93.3 1.7 %copy.25 = bf16[64,2048]{1,0:T(8,128)(2,1)} copy(bf16[64,2048]{1,0:T(8,128)(2,1)} %get-tuple-element.8) | data formatting | bytes 524288
  94.9 2.1 %copy.26 = f32[64,24,128]{2,1,0:T(8,128)} copy(f32[64,24,128]{2,1,0:T(8,128)} %bitcast.10) | data formatting | bytes 1572864

commit v2 on v1

--- a/solution.py
+++ b/solution.py
@@ -18,6 +18,10 @@
 
 def dot(a, b):
     return jnp.dot(a, b, preferred_element_type=F32)
+
+
+def dot_t(a, b):
+    return lax.dot_general(a, b, (((1,), (1,)), ((), ())), preferred_element_type=F32)
 
 
 def chip_offsets(chips):
@@ -112,8 +116,8 @@
     lanes = 2 * entries
     groups = decay_v.shape[0]
     group_width = b_v.shape[0] // groups
-    experts = wexp_v.shape[1]
-    egroups = wgrp_v.shape[1]
+    experts = wexp_v.shape[0]
+    egroups = wgrp_v.shape[0]
     local_experts = wg_v.shape[0]
     cap = z_buf.shape[1] // local_experts
     slots = z_buf.shape[1]
@@ -149,8 +153,8 @@
         ("wout", wout_h, wout_v),
         ("gmix", gmix_h.at[:, share_at], gmix_v),
         ("routes", routes_h, routes_v),
-        ("wgrp", wgrp_h.at[share_at, :], wgrp_v),
-        ("wexp", wexp_h.at[share_at, :], wexp_v),
+        ("wgrp", wgrp_h.at[:, share_at], wgrp_v),
+        ("wexp", wexp_h.at[:, share_at], wexp_v),
         ("wg", wg_h, wg_v),
         ("wu", wu_h, wu_v),
         ("wd", wd_h, wd_v),
@@ -239,13 +243,8 @@
             news.append(new.astype(BF16))
         c_j = c_v[channels, :] * sign
         c_wide = jnp.where(own_group, jnp.concatenate([c_j] * per_block, axis=1), 0.0)
-        y = lax.dot_general(
-            jnp.concatenate(news, axis=1),
-            c_wide.astype(BF16),
-            (((1,), (1,)), ((), ())),
-            preferred_element_type=F32,
-        )
-        y = y + skip_v[:, channels] * u_j.astype(F32)
+        y = dot_t(jnp.concatenate(news, axis=1), c_wide.astype(BF16))
+        y = y + skip_v[j : j + 1, :] * u_j.astype(F32)
         acts.append(jax.nn.gelu(y).astype(BF16))
     store = pltpu.make_async_copy(ns_v, ns_h, store_sem)
     store.start()
@@ -265,8 +264,20 @@
 
     for name in ("routes", "gmix", "wgrp", "wexp"):
         loads[name].wait()
-    route = [routes_v[:, k : k + 1] for k in range(2)]
-    expert_id = lax.broadcasted_iota(jnp.int32, (rows, experts), 1)
+    route = [
+        jnp.sum(
+            jnp.where(
+                lax.broadcasted_iota(jnp.int32, (rows, rows), 0)
+                == lax.broadcasted_iota(jnp.int32, (rows, rows), 1),
+                routes_v[k : k + 1, :].astype(F32),
+                0.0,
+            ),
+            axis=1,
+            keepdims=True,
+        )
+        for k in range(2)
+    ]
+    expert_id = lax.broadcasted_iota(jnp.int32, (rows, experts), 1).astype(F32)
     chosen = [(route[k] == expert_id).astype(F32) for k in range(2)]
     hits = chosen[0] + chosen[1]
     row_id = lax.broadcasted_iota(jnp.int32, (rows, rows), 0)
@@ -277,7 +288,7 @@
     places = []
     for k in range(2):
         rank = jnp.sum(prior * chosen[k], axis=1, keepdims=True)
-        target = route[k].astype(F32) * cap + rank
+        target = route[k] * cap + rank
         places.append((target == slot_id).astype(F32))
     dispatch_map = (places[0] + places[1]).astype(BF16)
 
@@ -356,8 +367,8 @@
                     {"ep": target},
                 )
 
-    group_logit = dot(hidden_bf, wgrp_v[...])
-    expert_logit = dot(hidden_bf, wexp_v[...])
+    group_logit = dot_t(hidden_bf, wgrp_v[...])
+    expert_logit = dot_t(hidden_bf, wexp_v[...])
     columns = [jnp.sum(chosen[k] * expert_logit, axis=1, keepdims=True) for k in range(2)]
     columns += [group_logit[:, i : i + 1] for i in range(egroups)]
     exchange(1, columns)
@@ -444,8 +455,13 @@
     total = [sum(p[i] for p in parts) for i in range(2 + egroups)]
     pair = [jnp.exp(total[k]) for k in range(2)]
     group_exp = [jnp.exp(total[2 + i]) for i in range(egroups)]
-    own = route[0] // (experts // egroups)
-    picked = sum(jnp.where(own == i, group_exp[i], 0.0) for i in range(egroups))
+    group_size = experts // egroups
+    picked = sum(
+        jnp.where(
+            (route[0] >= i * group_size) & (route[0] < (i + 1) * group_size), group_exp[i], 0.0
+        )
+        for i in range(egroups)
+    )
     group_prob = picked / sum(group_exp)
     pair_sum = pair[0] + pair[1]
     combine_map = sum(places[k] * (pair[k] / pair_sum * group_prob) for k in range(2))
@@ -516,18 +532,18 @@
     args = (
         x_in,
         state.reshape(rows * groups, lanes),
-        routes,
+        routes.T,
         w_in,
         decay_rate,
         frequency,
         log_step.reshape(1, groups),
         b_in.reshape(channels, lanes),
         c_out.reshape(channels, lanes),
-        skip.reshape(1, channels),
+        skip.reshape(channels // lanes, lanes),
         w_out,
         gain_mix.reshape(1, width),
-        w_group,
-        w_expert,
+        w_group.T,
+        w_expert.T,
         w_gate,
         w_up,
         w_down.reshape(local_experts * hidden_units, width),
@@ -538,18 +554,18 @@
     scratch = [
         pltpu.VMEM((rows, width), BF16),
         pltpu.VMEM((rows * groups, lanes), F32),
-        pltpu.VMEM(routes.shape, jnp.int32),
+        pltpu.VMEM(routes.shape[::-1], jnp.int32),
         pltpu.VMEM(w_in.shape, BF16),
         pltpu.VMEM(decay_rate.shape, F32),
         pltpu.VMEM(frequency.shape, F32),
         pltpu.VMEM((1, groups), F32),
         pltpu.VMEM((channels, lanes), F32),
         pltpu.VMEM((channels, lanes), F32),
-        pltpu.VMEM((1, channels), F32),
+        pltpu.VMEM((channels // lanes, lanes), F32),
         pltpu.VMEM(w_out.shape, BF16),
         pltpu.VMEM((1, share), F32),
-        pltpu.VMEM((share, egroups), BF16),
-        pltpu.VMEM((share, experts), BF16),
+        pltpu.VMEM((egroups, share), BF16),
+        pltpu.VMEM((experts, share), BF16),
         pltpu.VMEM(w_gate.shape, BF16),
         pltpu.VMEM(w_up.shape, BF16),
         pltpu.VMEM((local_experts * hidden_units, width), BF16),

time: 98.6 us -> 92 us (0.933); the launches traced: 97 us -> 91.5 us
  local copies, waits for them, and re-layouts: 10.1 us -> 3.73 us
    unnamed x5 -> x2, local copies, waits for them, and re-layouts: 8.84 us -> 3.73 us
    reshape x1 -> x0, local copies, waits for them, and re-layouts: 1.26 us -> none  [per_device(): skip.reshape(1, channels)]
where the time goes in v2:
time: 92 us; the launch traced here: 91.5 us
  Pallas kernels  87.1 us (95%)
  local copies, waits for them, and re-layouts  3.73 us (4%)
    pallas_call x1, Pallas kernels, per_device(): pl.pallas_call(functools.partial(layer_kernel, n_ep, n_tp), out_shape=(ja...  87.1 us
    unnamed x2, local copies, waits for them, and re-layouts  3.73 us

profile of v2, /device:TPU:40, one launch (start us, length us, event | category | flops | bytes accessed | tf_op | source)
XLA Modules:
  0.0 91.5 jit_solution(14421207028906493759)
XLA Ops:
  0.6 87.1 %layer.1 = (bf16[64,2048]{1,0:T(8,128)(2,1)}, f32[1536,128]{1,0:T(8,128)}) custom-call(bf16[64,2048]{1,0:T(8,128)(2,1)} %x_h.1, f32[1536,128]{1,0:T(8,128)} %bitcast.13, s32[2,64]{1,0:T(2,128)} %bitcast.22, bf16[2048,384]{1,0:T(8,128)(2,1)} %win_h.1, f32[24,64]{1,0:T(8,128)} %decay_h.1, f32[24,64]{1,0:T(8,128)} %freq_h.1, f32[1,24]{1,0:T(1,128)} %bitcast.23, ...), custom_call_target="tpu_custom_call" | custom-call | tf_op jit(solution)/shard_map/layer/pallas_call | solution.py:605
  87.7 1.7 %copy.22 = bf16[64,2048]{1,0:T(8,128)(2,1)} copy(bf16[64,2048]{1,0:T(8,128)(2,1)} %get-tuple-element.8) | data formatting | bytes 524288
  89.4 2.1 %copy.23 = f32[64,24,128]{2,1,0:T(8,128)} copy(f32[64,24,128]{2,1,0:T(8,128)} %bitcast.14) | data formatting | bytes 1572864

commit v3 on v2

--- a/solution.py
+++ b/solution.py
@@ -25,12 +25,14 @@
 
 
 def chip_offsets(chips):
-    order = [0]
-    for step in range(1, chips // 2):
-        order += [step, chips - step]
-    order.append(chips // 2)
+    far_first = [chips // 2]
+    for step in range(chips // 2 - 1, 0, -1):
+        far_first += [step, chips - step]
+    far_first.append(0)
     size = chips // CHUNKS
-    return [order[k * size : (k + 1) * size] for k in range(CHUNKS)]
+    first = far_first[-1 - size : -1]
+    rest = far_first[: -1 - size] + [0]
+    return [first] + [rest[k * size : (k + 1) * size] for k in range(CHUNKS - 1)]
 
 
 def layer_kernel(
@@ -53,7 +55,6 @@
     wg_h,
     wu_h,
     wd_h,
-    gmoe_h,
     out_h,
     ns_h,
     x_v,
@@ -73,7 +74,6 @@
     wg_v,
     wu_v,
     wd_v,
-    gmoe_v,
     ns_v,
     out_part,
     out_recv,
@@ -126,19 +126,6 @@
     chunk_rows = per_chunk * slots
     share_at = pl.ds(pl.multiple_of(tp * share, share), share)
 
-    barrier = pltpu.get_barrier_semaphore()
-
-    def greet_ep(i, _):
-        peer = (ep + i) % n_ep
-        pl.semaphore_signal(barrier, inc=1, device_id={"ep": peer}, device_id_type=MESH)
-        return 0
-
-    for r in range(1, n_tp):
-        pl.semaphore_signal(
-            barrier, inc=1, device_id={"tp": (tp + r) % n_tp}, device_id_type=MESH
-        )
-    lax.fori_loop(1, n_ep, greet_ep, 0)
-
     loads = {}
     pairs = (
         ("x", x_h, x_v),
@@ -151,18 +138,31 @@
         ("state", state_h, state_v),
         ("skip", skip_h, skip_v),
         ("wout", wout_h, wout_v),
-        ("gmix", gmix_h.at[:, share_at], gmix_v),
+        ("gmix", gmix_h, gmix_v),
         ("routes", routes_h, routes_v),
         ("wgrp", wgrp_h.at[:, share_at], wgrp_v),
         ("wexp", wexp_h.at[:, share_at], wexp_v),
         ("wg", wg_h, wg_v),
         ("wu", wu_h, wu_v),
         ("wd", wd_h, wd_v),
-        ("gmoe", gmoe_h.at[:, share_at], gmoe_v),
     )
     for i, (name, src, dst) in enumerate(pairs):
         loads[name] = pltpu.make_async_copy(src, dst, load_sem.at[i])
         loads[name].start()
+
+    barrier = pltpu.get_barrier_semaphore()
+
+    def greet_ep(i, _):
+        step = n_ep // 2 + jnp.where(i % 2 == 0, i // 2, -(i // 2) - 1)
+        peer = (ep + step) % n_ep
+        pl.semaphore_signal(barrier, inc=1, device_id={"ep": peer}, device_id_type=MESH)
+        return 0
+
+    for r in range(1, n_tp):
+        pl.semaphore_signal(
+            barrier, inc=1, device_id={"tp": (tp + r) % n_tp}, device_id_type=MESH
+        )
+    lax.fori_loop(0, n_ep - 1, greet_ep, 0)
 
     sends = []
 
@@ -251,16 +251,20 @@
     act_mix = jnp.concatenate(acts, axis=1)
 
     loads["wout"].wait()
-    pl.semaphore_wait(barrier, n_ep - 1 + n_tp - 1)
-    waits = {}
     for r in (2, 1, 3, 0):
         q = (tp + r) % n_tp
         cols = pl.ds(pl.multiple_of(q * share, share), share)
         out_part[r] = dot(act_mix, wout_v[:, cols]).astype(BF16)
-        if r:
-            waits[r] = send(
-                out_part.at[r], out_recv.at[r - 1], a_send.at[r - 1], a_recv.at[r - 1], {"tp": q}
-            )
+    pl.semaphore_wait(barrier, n_ep - 1 + n_tp - 1)
+    waits = {}
+    for r in (2, 1, 3):
+        waits[r] = send(
+            out_part.at[r],
+            out_recv.at[r - 1],
+            a_send.at[r - 1],
+            a_recv.at[r - 1],
+            {"tp": (tp + r) % n_tp},
+        )
 
     for name in ("routes", "gmix", "wgrp", "wexp"):
         loads[name].wait()
@@ -325,34 +329,24 @@
             for part in parts
         ]
 
-    def norm_terms(n, values):
-        mean_own = jnp.mean(values, axis=1, keepdims=True)
-        spread_own = jnp.sum(jnp.square(values - mean_own), axis=1, keepdims=True)
-        exchange(n, [mean_own, spread_own])
-        stats = received(n, 2)
-        mean = sum(s[0] for s in stats) / n_tp
-        spread = sum(s[1] + share * jnp.square(s[0] - mean) for s in stats) / width
-        return mean, lax.rsqrt(spread + norm_eps)
+    shift = residual_scale * jnp.mean(x_v[...].astype(F32), axis=1, keepdims=True)
+    base = residual_scale * x_v[:, share_at].astype(F32) - shift
 
     for r in range(1, n_tp):
         waits[r].wait_recv()
     mixed = out_part[0].astype(F32)
     for r in range(1, n_tp):
         mixed = mixed + out_recv[r - 1].astype(F32)
-    values = residual_scale * x_v[:, share_at].astype(F32) + mixed
-    mean, scale = norm_terms(0, values)
-    hidden = (values - mean) * scale * gmix_v[...]
-    hid_v[...] = hidden
-    hidden_bf = hidden.astype(BF16)
+    values = base + mixed
 
     z_buf[...] = (
         lax.dot_general(
-            dispatch_map, hidden_bf, (((0,), (0,)), ((), ())), preferred_element_type=F32
+            dispatch_map, values.astype(BF16), (((0,), (0,)), ((), ())), preferred_element_type=F32
         )
         .reshape(n_ep, slots, share)
         .astype(BF16)
     )
-    z_recv_buf[0, core] = z_buf[ep]
+    z_recv_buf[CHUNKS - 1, per_chunk - CORES + core] = z_buf[ep]
     for k in range(CHUNKS):
         for i, offset in enumerate(offsets[k]):
             for c in (1, 0):
@@ -367,17 +361,16 @@
                     {"ep": target},
                 )
 
-    group_logit = dot_t(hidden_bf, wgrp_v[...])
-    expert_logit = dot_t(hidden_bf, wexp_v[...])
-    columns = [jnp.sum(chosen[k] * expert_logit, axis=1, keepdims=True) for k in range(2)]
-    columns += [group_logit[:, i : i + 1] for i in range(egroups)]
-    exchange(1, columns)
+    mean_own = jnp.mean(values, axis=1, keepdims=True)
+    spread_own = jnp.sum(jnp.square(values - mean_own), axis=1, keepdims=True)
+    exchange(0, [mean_own, spread_own])
+    hid_v[...] = values
 
     def wait_bytes(ref, sem):
         pltpu.make_async_copy(ref, ref, sem).wait()
 
     def gather(k):
-        count = per_chunk - 1 if k == 0 else per_chunk
+        count = per_chunk - 1 if k == CHUNKS - 1 else per_chunk
         wait_bytes(z_recv_buf.at[k, 0:count], z_recv.at[k])
         for r in (2, 1, 3):
             send(
@@ -395,8 +388,18 @@
         if k == 0:
             for name in ("wg", "wu", "wd"):
                 loads[name].wait()
-        lhs = [gather_buf[k, t].reshape(chunk_rows, share) for t in range(n_tp)]
-        lhs = jnp.concatenate(lhs, axis=1)
+        parts = [gather_buf[k, t].astype(F32).reshape(chunk_rows, share) for t in range(n_tp)]
+        mean = sum(jnp.sum(p, axis=1, keepdims=True) for p in parts) / width
+        parts = [p - mean for p in parts]
+        spread = sum(jnp.sum(jnp.square(p), axis=1, keepdims=True) for p in parts) / width
+        scale = lax.rsqrt(spread + norm_eps)
+        lhs = jnp.concatenate(
+            [
+                (p * scale * gmix_v[:, t * share : (t + 1) * share]).astype(BF16)
+                for t, p in enumerate(parts)
+            ],
+            axis=1,
+        )
         slot = lax.broadcasted_iota(jnp.int32, (chunk_rows, 1), 0) % slots
         acts = []
         for e in range(local_experts):
@@ -438,18 +441,34 @@
                     r_recv,
                     {"ep": target},
                 )
-        if k == 0:
-            ret_buf[ep] = ret_send[0, core]
+        if k == CHUNKS - 1:
+            ret_buf[ep] = ret_send[k, per_chunk - CORES + core]
 
     gather(0)
+
+    stats = received(0, 2)
+    mean = sum(s[0] for s in stats) / n_tp
+    spread = sum(s[1] + share * jnp.square(s[0] - mean) for s in stats) / width
+    hidden = (hid_v[...] - mean) * lax.rsqrt(spread + norm_eps) * gmix_v[:, share_at]
+    hid_v[...] = hidden
+    hidden_bf = hidden.astype(BF16)
+
+    group_logit = dot_t(hidden_bf, wgrp_v[...])
+    expert_logit = dot_t(hidden_bf, wexp_v[...])
+    columns = [jnp.sum(chosen[k] * expert_logit, axis=1, keepdims=True) for k in range(2)]
+    columns += [group_logit[:, i : i + 1] for i in range(egroups)]
+    exchange(1, columns)
+
+    experts_of(0)
     gather(1)
-    experts_of(0)
-    for k in range(2, CHUNKS):
-        gather(k)
-        experts_of(k - 1)
-        give_back(k - 2)
-    experts_of(CHUNKS - 1)
-    give_back(CHUNKS - 2)
+    give_back(0)
+    gather(2)
+    gather(3)
+    experts_of(1)
+    experts_of(2)
+    give_back(1)
+    experts_of(3)
+    give_back(2)
 
     parts = received(1, 2 + egroups)
     total = [sum(p[i] for p in parts) for i in range(2 + egroups)]
@@ -466,15 +485,13 @@
     pair_sum = pair[0] + pair[1]
     combine_map = sum(places[k] * (pair[k] / pair_sum * group_prob) for k in range(2))
     combine_map = combine_map.astype(BF16)
-    loads["gmoe"].wait()
 
     give_back(CHUNKS - 1)
 
     wait_bytes(ret_buf.at[0 : n_ep - 1], r_recv)
     returned = ret_buf[...].reshape(n_ep * slots, share)
     values = residual_scale * hid_v[...] + dot(combine_map, returned)
-    mean, scale = norm_terms(2, values)
-    fin_v[...] = ((values - mean) * scale * gmoe_v[...]).astype(BF16)
+    fin_v[...] = values.astype(BF16)
     last = []
     for r in (2, 1, 3):
         last.append(
@@ -494,6 +511,49 @@
     store.wait()
     for copy in sends:
         copy.wait_send()
+
+
+def finish_kernel(
+    pieces,
+    raw_h,
+    ns_h,
+    gain_h,
+    out_h,
+    new_h,
+    raw_v,
+    ns_v,
+    gain_v,
+    out_v,
+    load_sem,
+    store_sem,
+    in_sem,
+    out_sem,
+):
+    size = ns_v.shape[0] // pieces
+    raw = pltpu.make_async_copy(raw_h, raw_v, load_sem.at[0])
+    gain = pltpu.make_async_copy(gain_h, gain_v, load_sem.at[1])
+    raw.start()
+    gain.start()
+    ins, outs = [], []
+    for i in range(pieces):
+        part = pl.ds(i * size, size)
+        ins.append(pltpu.make_async_copy(ns_h.at[part], ns_v.at[part], in_sem.at[i]))
+        outs.append(pltpu.make_async_copy(ns_v.at[part], new_h.at[part], out_sem.at[i]))
+        ins[i].start()
+    raw.wait()
+    gain.wait()
+    values = raw_v[...].astype(F32)
+    centred = values - jnp.mean(values, axis=1, keepdims=True)
+    spread = jnp.mean(jnp.square(centred), axis=1, keepdims=True)
+    out_v[...] = (centred * lax.rsqrt(spread + norm_eps) * gain_v[...]).astype(BF16)
+    store = pltpu.make_async_copy(out_v, out_h, store_sem)
+    store.start()
+    for i in range(pieces):
+        ins[i].wait()
+        outs[i].start()
+    for copy in outs:
+        copy.wait()
+    store.wait()
 
 
 def per_device(
@@ -547,7 +607,6 @@
         w_gate,
         w_up,
         w_down.reshape(local_experts * hidden_units, width),
-        gain_moe.reshape(1, width),
     )
     dma = pltpu.SemaphoreType.DMA
     peers = n_tp - 1
@@ -563,19 +622,18 @@
         pltpu.VMEM((channels, lanes), F32),
         pltpu.VMEM((channels // lanes, lanes), F32),
         pltpu.VMEM(w_out.shape, BF16),
-        pltpu.VMEM((1, share), F32),
+        pltpu.VMEM((1, width), F32),
         pltpu.VMEM((egroups, share), BF16),
         pltpu.VMEM((experts, share), BF16),
         pltpu.VMEM(w_gate.shape, BF16),
         pltpu.VMEM(w_up.shape, BF16),
         pltpu.VMEM((local_experts * hidden_units, width), BF16),
-        pltpu.VMEM((1, share), F32),
         pltpu.VMEM((rows * groups, lanes), F32),
         pltpu.VMEM((n_tp, rows, share), BF16),
         pltpu.VMEM((peers, rows, share), BF16),
         pltpu.VMEM((rows, share), F32),
-        pltpu.VMEM((3, 8, 128), F32),
-        pltpu.VMEM((3, peers, 8, 128), F32),
+        pltpu.VMEM((2, 8, 128), F32),
+        pltpu.VMEM((2, peers, 8, 128), F32),
         pltpu.VMEM((n_ep, slots, share), BF16),
         pltpu.VMEM((CHUNKS, per_chunk, slots, share), BF16),
         pltpu.VMEM((CHUNKS, n_tp, per_chunk, slots, share), BF16),
@@ -588,8 +646,8 @@
         dma,
         dma((peers,)),
         dma((peers,)),
-        dma((3, peers)),
-        dma((3, peers)),
+        dma((2, peers)),
+        dma((2, peers)),
         dma((n_ep,)),
         dma((CHUNKS,)),
         dma((CHUNKS, peers)),
@@ -602,7 +660,7 @@
         dma((peers,)),
     ]
     any_space = pl.BlockSpec(memory_space=pl.ANY)
-    out, new_state = pl.pallas_call(
+    raw, new_state = pl.pallas_call(
         functools.partial(layer_kernel, n_ep, n_tp),
         out_shape=(
             jax.ShapeDtypeStruct((rows, width), BF16),
@@ -616,6 +674,27 @@
         ),
         name="layer",
     )(*args)
+    pieces = 4
+    out, new_state = pl.pallas_call(
+        functools.partial(finish_kernel, pieces),
+        out_shape=(
+            jax.ShapeDtypeStruct((rows, width), BF16),
+            jax.ShapeDtypeStruct((rows * groups, lanes), F32),
+        ),
+        in_specs=[any_space] * 3,
+        out_specs=(any_space, any_space),
+        scratch_shapes=[
+            pltpu.VMEM((rows, width), BF16),
+            pltpu.VMEM((rows * groups, lanes), F32),
+            pltpu.VMEM((1, width), F32),
+            pltpu.VMEM((rows, width), BF16),
+            dma((2,)),
+            dma,
+            dma((pieces,)),
+            dma((pieces,)),
+        ],
+        name="finish",
+    )(raw, new_state, gain_moe.reshape(1, width))
     return out, new_state.reshape(state.shape)
 
 

time: 92 us -> 83.1 us (0.903)
  Pallas kernels: 87.1 us -> 82.3 us
  local copies, waits for them, and re-layouts: 3.73 us -> 0 us
    pallas_call x1, Pallas kernels: 87.1 us -> 79.8 us  [per_device(): pl.pallas_call(functools.partial(layer_kernel, n_ep, n_tp), out_shape=(ja...]
    unnamed x2 -> x0, local copies, waits for them, and re-layouts: 3.73 us -> none
    pallas_call x0 -> x1, Pallas kernels: none -> 2.46 us  [per_device(): pl.pallas_call(functools.partial(finish_kernel, pieces), out_shape=(jax.S...]
where the time goes in v3:
time: 83.1 us; the launch traced here: 82.9 us
  Pallas kernels  82.3 us (99%)
    pallas_call x1, Pallas kernels, per_device(): pl.pallas_call(functools.partial(layer_kernel, n_ep, n_tp), out_shape=(ja...  79.8 us
    pallas_call x1, Pallas kernels, per_device(): pl.pallas_call(functools.partial(finish_kernel, pieces), out_shape=(jax.S...  2.46 us

profile of v3, /device:TPU:40, one launch (start us, length us, event | category | flops | bytes accessed | tf_op | source)
XLA Modules:
  0.0 82.9 jit_solution(6660180661610815353)
XLA Ops:
  0.6 79.8 %layer.1 = (bf16[64,2048]{1,0:T(8,128)(2,1)}, f32[1536,128]{1,0:T(8,128)}) custom-call(bf16[64,2048]{1,0:T(8,128)(2,1)} %x_h.1, f32[1536,128]{1,0:T(8,128)} %bitcast.13, s32[2,64]{1,0:T(2,128)} %bitcast.21, bf16[2048,384]{1,0:T(8,128)(2,1)} %win_h.1, f32[24,64]{1,0:T(8,128)} %decay_h.1, f32[24,64]{1,0:T(8,128)} %freq_h.1, f32[1,24]{1,0:T(1,128)} %bitcast.22, ...), custom_call_target="tpu_custom_call" | custom-call | tf_op jit(solution)/shard_map/layer/pallas_call | solution.py:663
  80.5 2.5 %finish.1 = (bf16[64,2048]{1,0:T(8,128)(2,1)}, f32[1536,128]{1,0:T(8,128)}) custom-call(bf16[64,2048]{1,0:T(8,128)(2,1)} %get-tuple-element.6.raw_h, f32[1536,128]{1,0:T(8,128)} %get-tuple-element.7.ns_h, f32[1,2048]{1,0:T(1,128)} %bitcast.19), custom_call_target="tpu_custom_call" | custom-call | tf_op jit(solution)/shard_map/finish/pallas_call | solution.py:678

commit v4 on v3

--- a/solution.py
+++ b/solution.py
@@ -10,7 +10,9 @@
 residual_scale = 8.0**0.25
 norm_eps = 1e-05
 CORES = 2
-CHUNKS = 4
+NEAR = 1
+ARC = 5
+SCHEDULE = ("D0", "D1", "G0", "H0", "E0", "G1", "G2", "B0", "E1", "G3", "E2", "B1", "E3", "B2", "W0", "B3")
 F32 = jnp.float32
 BF16 = jnp.bfloat16
 MESH = pl.DeviceIdType.MESH
@@ -22,17 +24,6 @@
 
 def dot_t(a, b):
     return lax.dot_general(a, b, (((1,), (1,)), ((), ())), preferred_element_type=F32)
-
-
-def chip_offsets(chips):
-    far_first = [chips // 2]
-    for step in range(chips // 2 - 1, 0, -1):
-        far_first += [step, chips - step]
-    far_first.append(0)
-    size = chips // CHUNKS
-    first = far_first[-1 - size : -1]
-    rest = far_first[: -1 - size] + [0]
-    return [first] + [rest[k * size : (k + 1) * size] for k in range(CHUNKS - 1)]
 
 
 def layer_kernel(
@@ -102,8 +93,9 @@
     d_recv,
     r_send,
     r_recv,
-    f_send,
-    f_recv,
+    l_send,
+    l_recv,
+    o_send,
 ):
     ep = lax.axis_index("ep")
     tp = lax.axis_index("tp")
@@ -121,9 +113,23 @@
     local_experts = wg_v.shape[0]
     cap = z_buf.shape[1] // local_experts
     slots = z_buf.shape[1]
-    offsets = chip_offsets(chips)
-    per_chunk = n_ep // CHUNKS
-    chunk_rows = per_chunk * slots
+    arc = chips - 2 * NEAR - 1
+    near = [offset for step in range(1, NEAR + 1) for offset in (step, -step)] + [0]
+    far = sorted(range(NEAR + 1, chips - NEAR), key=lambda offset: abs(offset - chips // 2))
+    counts = [len(near) * CORES]
+    counts += [min(ARC, arc - i) * CORES for i in range(0, arc, ARC)]
+    chunks = len(counts)
+    starts = [sum(counts[:k]) for k in range(chunks)]
+    blocks = [pl.ds(starts[k], counts[k]) for k in range(chunks)]
+    sums = [pl.ds(starts[k] * slots, counts[k] * slots) for k in range(chunks)]
+    remote = [counts[0] - 1] + counts[1:]
+    home = len(near) * CORES - CORES + core
+
+    def wrapped(host):
+        after = (host + chips - NEAR - 1) % chips
+        return (chips - NEAR - 1 - host) * (1 - after // (arc - 1))
+
+    right, left, opposite = (tp + 1) % n_tp, (tp + n_tp - 1) % n_tp, (tp + 2) % n_tp
     share_at = pl.ds(pl.multiple_of(tp * share, share), share)
 
     loads = {}
@@ -164,8 +170,6 @@
         )
     lax.fori_loop(0, n_ep - 1, greet_ep, 0)
 
-    sends = []
-
     def send(src, dst, send_sem, recv_sem, target):
         copy = pltpu.make_async_remote_copy(
             src_ref=src,
@@ -176,8 +180,10 @@
             device_id_type=MESH,
         )
         copy.start()
-        sends.append(copy)
         return copy
+
+    def wait_bytes(ref, sem):
+        pltpu.make_async_copy(ref, ref, sem).wait()
 
     for name in ("decay", "freq", "lstep", "b", "c"):
         loads[name].wait()
@@ -346,18 +352,24 @@
         .reshape(n_ep, slots, share)
         .astype(BF16)
     )
-    z_recv_buf[CHUNKS - 1, per_chunk - CORES + core] = z_buf[ep]
-    for k in range(CHUNKS):
-        for i, offset in enumerate(offsets[k]):
+    z_recv_buf[home] = z_buf[ep]
+    def dispatch(k):
+        for i, offset in enumerate(far if k else near):
+            host = (chip + chips - offset) % chips
+            if k:
+                rank = (offset - NEAR - 1 + arc - wrapped(host)) % arc
+                place, chunk = starts[1] + rank * CORES + core, 1 + rank // ARC
+            else:
+                place, chunk = i * CORES + core, 0
             for c in (1, 0):
                 if offset == 0 and c == 0:
                     continue
-                target = ((chip + chips - offset) % chips) * CORES + (core + c) % CORES
+                target = host * CORES + (core + c) % CORES
                 send(
                     z_buf.at[target],
-                    z_recv_buf.at[k, i * CORES + core],
-                    z_send.at[(k * len(offsets[k]) + i) * CORES + c],
-                    z_recv.at[k],
+                    z_recv_buf.at[place],
+                    z_send.at[k],
+                    z_recv.at[chunk],
                     {"ep": target},
                 )
 
@@ -366,29 +378,27 @@
     exchange(0, [mean_own, spread_own])
     hid_v[...] = values
 
-    def wait_bytes(ref, sem):
-        pltpu.make_async_copy(ref, ref, sem).wait()
-
     def gather(k):
-        count = per_chunk - 1 if k == CHUNKS - 1 else per_chunk
-        wait_bytes(z_recv_buf.at[k, 0:count], z_recv.at[k])
-        for r in (2, 1, 3):
+        wait_bytes(z_recv_buf.at[0 : remote[k]], z_recv.at[k])
+        peers = ((2, opposite), (1, left), (0, right))
+        for n, peer in peers:
             send(
-                z_recv_buf.at[k],
-                gather_buf.at[k, tp],
-                x_send.at[k, r - 1],
-                x_recv.at[k, r - 1],
-                {"tp": (tp + r) % n_tp},
+                z_recv_buf.at[blocks[k]],
+                gather_buf.at[tp, blocks[k]],
+                x_send.at[k],
+                x_recv.at[k, n],
+                {"tp": peer},
             )
-        gather_buf[k, tp] = z_recv_buf[k]
+        gather_buf[tp, blocks[k]] = z_recv_buf[blocks[k]]
 
     def experts_of(k):
-        for r in range(1, n_tp):
-            wait_bytes(gather_buf.at[k, 0], x_recv.at[k, r - 1])
+        for n in range(3):
+            wait_bytes(gather_buf.at[0, blocks[k]], x_recv.at[k, n])
         if k == 0:
             for name in ("wg", "wu", "wd"):
                 loads[name].wait()
-        parts = [gather_buf[k, t].astype(F32).reshape(chunk_rows, share) for t in range(n_tp)]
+        rows_k = counts[k] * slots
+        parts = [gather_buf[t, blocks[k]].astype(F32).reshape(rows_k, share) for t in range(n_tp)]
         mean = sum(jnp.sum(p, axis=1, keepdims=True) for p in parts) / width
         parts = [p - mean for p in parts]
         spread = sum(jnp.sum(jnp.square(p), axis=1, keepdims=True) for p in parts) / width
@@ -400,7 +410,7 @@
             ],
             axis=1,
         )
-        slot = lax.broadcasted_iota(jnp.int32, (chunk_rows, 1), 0) % slots
+        slot = lax.broadcasted_iota(jnp.int32, (rows_k, 1), 0) % slots
         acts = []
         for e in range(local_experts):
             gate = dot(lhs, wg_v[e])
@@ -411,106 +421,112 @@
         for r in (2, 1, 3, 0):
             q = (tp + r) % n_tp
             cols = pl.ds(pl.multiple_of(q * share, share), share)
-            down_part[k, r] = dot(act, wd_v[:, cols]).astype(BF16)
+            down_part[r, sums[k]] = dot(act, wd_v[:, cols]).astype(BF16)
             if r:
                 send(
-                    down_part.at[k, r],
-                    down_recv.at[k, r - 1],
-                    d_send.at[k, r - 1],
+                    down_part.at[r, sums[k]],
+                    down_recv.at[r - 1, sums[k]],
+                    d_send.at[k],
                     d_recv.at[k, r - 1],
                     {"tp": q},
                 )
 
     def give_back(k):
-        for r in range(1, n_tp):
-            wait_bytes(down_recv.at[k, r - 1], d_recv.at[k, r - 1])
-        total = down_part[k, 0].astype(F32)
-        for r in range(1, n_tp):
-            total = total + down_recv[k, r - 1].astype(F32)
-        ret_send[k] = total.reshape(per_chunk, slots, share).astype(BF16)
-        for i, offset in enumerate(offsets[k]):
+        for n in range(3):
+            wait_bytes(down_recv.at[n, sums[k]], d_recv.at[k, n])
+        total = down_part[0, sums[k]].astype(F32)
+        for n in range(3):
+            total = total + down_recv[n, sums[k]].astype(F32)
+        ret_send[blocks[k]] = total.reshape(counts[k], slots, share).astype(BF16)
+        for i in range(counts[k] // CORES):
+            if k:
+                rank = (k - 1) * ARC + i
+                source = (chip + NEAR + 1 + (rank + wrapped(chip)) % arc) % chips
+            else:
+                source = (chip + chips + near[i]) % chips
             for c in (1, 0):
                 to_core = (core + c) % CORES
-                if offset == 0 and c == 0:
+                if k == 0 and near[i] == 0 and c == 0:
+                    ret_buf[ep] = ret_send[home]
                     continue
-                target = ((chip + offset) % chips) * CORES + to_core
                 send(
-                    ret_send.at[k, i * CORES + to_core],
+                    ret_send.at[starts[k] + i * CORES + to_core],
                     ret_buf.at[ep],
-                    r_send.at[(k * len(offsets[k]) + i) * CORES + c],
+                    r_send.at[k],
                     r_recv,
-                    {"ep": target},
+                    {"ep": source * CORES + to_core},
                 )
-        if k == CHUNKS - 1:
-            ret_buf[ep] = ret_send[k, per_chunk - CORES + core]
-
-    gather(0)
-
-    stats = received(0, 2)
-    mean = sum(s[0] for s in stats) / n_tp
-    spread = sum(s[1] + share * jnp.square(s[0] - mean) for s in stats) / width
-    hidden = (hid_v[...] - mean) * lax.rsqrt(spread + norm_eps) * gmix_v[:, share_at]
-    hid_v[...] = hidden
-    hidden_bf = hidden.astype(BF16)
-
-    group_logit = dot_t(hidden_bf, wgrp_v[...])
-    expert_logit = dot_t(hidden_bf, wexp_v[...])
-    columns = [jnp.sum(chosen[k] * expert_logit, axis=1, keepdims=True) for k in range(2)]
-    columns += [group_logit[:, i : i + 1] for i in range(egroups)]
-    exchange(1, columns)
-
-    experts_of(0)
-    gather(1)
-    give_back(0)
-    gather(2)
-    gather(3)
-    experts_of(1)
-    experts_of(2)
-    give_back(1)
-    experts_of(3)
-    give_back(2)
-
-    parts = received(1, 2 + egroups)
-    total = [sum(p[i] for p in parts) for i in range(2 + egroups)]
-    pair = [jnp.exp(total[k]) for k in range(2)]
-    group_exp = [jnp.exp(total[2 + i]) for i in range(egroups)]
-    group_size = experts // egroups
-    picked = sum(
-        jnp.where(
-            (route[0] >= i * group_size) & (route[0] < (i + 1) * group_size), group_exp[i], 0.0
+
+    def router(k):
+        stats = received(0, 2)
+        mean = sum(s[0] for s in stats) / n_tp
+        spread = sum(s[1] + share * jnp.square(s[0] - mean) for s in stats) / width
+        hidden = (hid_v[...] - mean) * lax.rsqrt(spread + norm_eps) * gmix_v[:, share_at]
+        hid_v[...] = hidden
+        hidden_bf = hidden.astype(BF16)
+
+        group_logit = dot_t(hidden_bf, wgrp_v[...])
+        expert_logit = dot_t(hidden_bf, wexp_v[...])
+        columns = [jnp.sum(chosen[k] * expert_logit, axis=1, keepdims=True) for k in range(2)]
+        columns += [group_logit[:, i : i + 1] for i in range(egroups)]
+        exchange(1, columns)
+
+    weights = []
+
+    def route_weights(k):
+        parts = received(1, 2 + egroups)
+        total = [sum(p[i] for p in parts) for i in range(2 + egroups)]
+        pair = [jnp.exp(total[k]) for k in range(2)]
+        group_exp = [jnp.exp(total[2 + i]) for i in range(egroups)]
+        group_size = experts // egroups
+        picked = sum(
+            jnp.where(
+                (route[0] >= i * group_size) & (route[0] < (i + 1) * group_size), group_exp[i], 0.0
+            )
+            for i in range(egroups)
         )
-        for i in range(egroups)
-    )
-    group_prob = picked / sum(group_exp)
-    pair_sum = pair[0] + pair[1]
-    combine_map = sum(places[k] * (pair[k] / pair_sum * group_prob) for k in range(2))
-    combine_map = combine_map.astype(BF16)
-
-    give_back(CHUNKS - 1)
-
+        group_prob = picked / sum(group_exp)
+        pair_sum = pair[0] + pair[1]
+        combine_map = sum(places[k] * (pair[k] / pair_sum * group_prob) for k in range(2))
+        weights.append(combine_map.astype(BF16))
+
+    steps = {
+        "D": dispatch,
+        "G": gather,
+        "H": router,
+        "E": experts_of,
+        "W": route_weights,
+        "B": give_back,
+    }
+    for step in SCHEDULE:
+        steps[step[0]](int(step[1]))
+
+    for r in range(1, n_tp):
+        wait_bytes(out_recv.at[0], a_send.at[r - 1])
+        for n in range(2):
+            wait_bytes(stat_send.at[n], s_send.at[n, r - 1])
+    wait_bytes(z_recv_buf.at[0 : remote[0]], z_send.at[0])
+    wait_bytes(z_recv_buf.at[0 : sum(remote[1:])], z_send.at[1])
+    for k in range(chunks):
+        wait_bytes(gather_buf.at[0:3, blocks[k]], x_send.at[k])
+        wait_bytes(down_recv.at[0:3, sums[k]], d_send.at[k])
     wait_bytes(ret_buf.at[0 : n_ep - 1], r_recv)
     returned = ret_buf[...].reshape(n_ep * slots, share)
-    values = residual_scale * hid_v[...] + dot(combine_map, returned)
+    values = residual_scale * hid_v[...] + dot(weights[0], returned)
     fin_v[...] = values.astype(BF16)
-    last = []
     for r in (2, 1, 3):
-        last.append(
-            send(
-                fin_v,
-                out_h.at[:, share_at],
-                f_send.at[r - 1],
-                f_recv.at[r - 1],
-                {"tp": (tp + r) % n_tp},
-            )
+        send(
+            fin_v, out_h.at[:, share_at], l_send, l_recv.at[r - 1], {"tp": (tp + r) % n_tp}
         )
-    own_store = pltpu.make_async_copy(fin_v, out_h.at[:, share_at], f_send.at[n_tp - 1])
+    own_store = pltpu.make_async_copy(fin_v, out_h.at[:, share_at], o_send)
     own_store.start()
-    for copy in last:
-        copy.wait_recv()
+    for k in range(chunks):
+        wait_bytes(ret_buf.at[0 : remote[k]], r_send.at[k])
+    store.wait()
+    for r in range(1, n_tp):
+        wait_bytes(fin_v, l_recv.at[r - 1])
     own_store.wait()
-    store.wait()
-    for copy in sends:
-        copy.wait_send()
+    wait_bytes(out_recv, l_send)
 
 
 def finish_kernel(
@@ -588,7 +604,6 @@
     local_experts, _, hidden_units = w_gate.shape
     cap = max(2, 4 * rows // experts)
     slots = local_experts * cap
-    per_chunk = n_ep // CHUNKS
     args = (
         x_in,
         state.reshape(rows * groups, lanes),
@@ -610,6 +625,7 @@
     )
     dma = pltpu.SemaphoreType.DMA
     peers = n_tp - 1
+    chunks = 1 + pl.cdiv(n_ep // CORES - 2 * NEAR - 1, ARC)
     scratch = [
         pltpu.VMEM((rows, width), BF16),
         pltpu.VMEM((rows * groups, lanes), F32),
@@ -635,11 +651,11 @@
         pltpu.VMEM((2, 8, 128), F32),
         pltpu.VMEM((2, peers, 8, 128), F32),
         pltpu.VMEM((n_ep, slots, share), BF16),
-        pltpu.VMEM((CHUNKS, per_chunk, slots, share), BF16),
-        pltpu.VMEM((CHUNKS, n_tp, per_chunk, slots, share), BF16),
-        pltpu.VMEM((CHUNKS, n_tp, per_chunk * slots, share), BF16),
-        pltpu.VMEM((CHUNKS, peers, per_chunk * slots, share), BF16),
-        pltpu.VMEM((CHUNKS, per_chunk, slots, share), BF16),
+        pltpu.VMEM((n_ep, slots, share), BF16),
+        pltpu.VMEM((n_tp, n_ep, slots, share), BF16),
+        pltpu.VMEM((n_tp, n_ep * slots, share), BF16),
+        pltpu.VMEM((peers, n_ep * slots, share), BF16),
+        pltpu.VMEM((n_ep, slots, share), BF16),
         pltpu.VMEM((n_ep, slots, share), BF16),
         pltpu.VMEM((rows, share), BF16),
         dma((len(args),)),
@@ -648,16 +664,17 @@
         dma((peers,)),
         dma((2, peers)),
         dma((2, peers)),
-        dma((n_ep,)),
-        dma((CHUNKS,)),
-        dma((CHUNKS, peers)),
-        dma((CHUNKS, peers)),
-        dma((CHUNKS, peers)),
-        dma((CHUNKS, peers)),
-        dma((n_ep,)),
+        dma((2,)),
+        dma((chunks,)),
+        dma((chunks,)),
+        dma((chunks, peers)),
+        dma((chunks,)),
+        dma((chunks, peers)),
+        dma((chunks,)),
         dma,
-        dma((n_tp,)),
+        dma,
         dma((peers,)),
+        dma,
     ]
     any_space = pl.BlockSpec(memory_space=pl.ANY)
     raw, new_state = pl.pallas_call(

time: 83.1 us -> 78.3 us (0.942)
  Pallas kernels: 82.3 us -> 77.5 us
    pallas_call x1, Pallas kernels: 79.8 us -> 75 us  [per_device(): pl.pallas_call(functools.partial(layer_kernel, n_ep, n_tp), out_shape=(ja...]
where the time goes in v4:
time: 78.3 us; the launch traced here: 78.2 us
  Pallas kernels  77.5 us (99%)
    pallas_call x1, Pallas kernels, per_device(): pl.pallas_call(functools.partial(layer_kernel, n_ep, n_tp), out_shape=(ja...  75 us
    pallas_call x1, Pallas kernels, per_device(): pl.pallas_call(functools.partial(finish_kernel, pieces), out_shape=(jax.S...  2.46 us

profile of v4, /device:TPU:40, one launch (start us, length us, event | category | flops | bytes accessed | tf_op | source)
XLA Modules:
  0.0 78.2 jit_solution(11752348916743320718)
XLA Ops:
  0.6 75.0 %layer.1 = (bf16[64,2048]{1,0:T(8,128)(2,1)}, f32[1536,128]{1,0:T(8,128)}) custom-call(bf16[64,2048]{1,0:T(8,128)(2,1)} %x_h.1, f32[1536,128]{1,0:T(8,128)} %bitcast.13, s32[2,64]{1,0:T(2,128)} %bitcast.21, bf16[2048,384]{1,0:T(8,128)(2,1)} %win_h.1, f32[24,64]{1,0:T(8,128)} %decay_h.1, f32[24,64]{1,0:T(8,128)} %freq_h.1, f32[1,24]{1,0:T(1,128)} %bitcast.22, ...), custom_call_target="tpu_custom_call" | custom-call | tf_op jit(solution)/shard_map/layer/pallas_call | solution.py:680
  75.7 2.5 %finish.1 = (bf16[64,2048]{1,0:T(8,128)(2,1)}, f32[1536,128]{1,0:T(8,128)}) custom-call(bf16[64,2048]{1,0:T(8,128)(2,1)} %get-tuple-element.6.raw_h, f32[1536,128]{1,0:T(8,128)} %get-tuple-element.7.ns_h, f32[1,2048]{1,0:T(1,128)} %bitcast.19), custom_call_target="tpu_custom_call" | custom-call | tf_op jit(solution)/shard_map/finish/pallas_call | solution.py:695

commit v5 on v4

--- a/solution.py
+++ b/solution.py
@@ -168,7 +168,7 @@
         pl.semaphore_signal(
             barrier, inc=1, device_id={"tp": (tp + r) % n_tp}, device_id_type=MESH
         )
-    lax.fori_loop(0, n_ep - 1, greet_ep, 0)
+    lax.fori_loop(0, n_ep - 1, greet_ep, 0, unroll=True)
 
     def send(src, dst, send_sem, recv_sem, target):
         copy = pltpu.make_async_remote_copy(

time: 78.3 us -> 78.1 us (level)
  no operation moved by 1% of the time
where the time goes in v5:
time: 78.1 us; the launch traced here: 78 us
  Pallas kernels  77.3 us (99%)
    pallas_call x1, Pallas kernels, per_device(): pl.pallas_call(functools.partial(layer_kernel, n_ep, n_tp), out_shape=(ja...  74.9 us
    pallas_call x1, Pallas kernels, per_device(): pl.pallas_call(functools.partial(finish_kernel, pieces), out_shape=(jax.S...  2.46 us

profile of v5, /device:TPU:40, one launch (start us, length us, event | category | flops | bytes accessed | tf_op | source)
XLA Modules:
  0.0 78.0 jit_solution(17336364054229310208)
XLA Ops:
  0.6 74.9 %layer.1 = (bf16[64,2048]{1,0:T(8,128)(2,1)}, f32[1536,128]{1,0:T(8,128)}) custom-call(bf16[64,2048]{1,0:T(8,128)(2,1)} %x_h.1, f32[1536,128]{1,0:T(8,128)} %bitcast.13, s32[2,64]{1,0:T(2,128)} %bitcast.21, bf16[2048,384]{1,0:T(8,128)(2,1)} %win_h.1, f32[24,64]{1,0:T(8,128)} %decay_h.1, f32[24,64]{1,0:T(8,128)} %freq_h.1, f32[1,24]{1,0:T(1,128)} %bitcast.22, ...), custom_call_target="tpu_custom_call" | custom-call | tf_op jit(solution)/shard_map/layer/pallas_call | solution.py:680
  75.5 2.5 %finish.1 = (bf16[64,2048]{1,0:T(8,128)(2,1)}, f32[1536,128]{1,0:T(8,128)}) custom-call(bf16[64,2048]{1,0:T(8,128)(2,1)} %get-tuple-element.6.raw_h, f32[1536,128]{1,0:T(8,128)} %get-tuple-element.7.ns_h, f32[1,2048]{1,0:T(1,128)} %bitcast.19), custom_call_target="tpu_custom_call" | custom-call | tf_op jit(solution)/shard_map/finish/pallas_call | solution.py:695
